TPU v7x, 512 devices: a whole 4x8x8 slice. The times are simulated.
512 devices in a mesh: fs: 64 (over z, y), rep: 4 (over x), tp: 2 (over core).
Axes of the slice: x: 4, y: 8, z: 8, core: 2. Of those that a mesh axis runs over, the one named last changes fastest.
Arguments:
- tokens_in: bfloat16 [131072, 2048], P(('fs', 'rep')), may hold values from -24 to 24
- query_two: bfloat16 [131072, 512], P(('fs', 'rep'), 'tp'), may hold values from -49 to 49
- key_two: bfloat16 [131072, 512], P(('fs', 'rep'), 'tp'), may hold values from -9 to 9
- values: bfloat16 [131072, 1024], P(('fs', 'rep'), 'tp'), may hold values from -6 to 6
- out_grad: bfloat16 [131072, 1024], P(('fs', 'rep'), 'tp'), may hold values from -6 to 6
- second_scale: float32 [8], P('tp'), may hold values from 0.3 to 0.8
- factor: bfloat16 [2048, 256], P('fs'), may hold values from -0.125 to 0.125
- weight: float32 [2048, 512], P('fs', 'tp'), may hold values from -0.6 to 0.6
- first_moment: float32 [256, 512], P('fs', 'tp'), may hold values from -543.058 to 543.058
- second_moment: float32 [256, 512], P('fs', 'tp'), may hold values from 81 to 131072
Outputs:
- new_weight: float32 [2048, 512], P('fs', 'tp')
- weight_copy: bfloat16 [2048, 512], P(None, 'tp')
- update_step: float32 [2048, 512], P('fs', 'tp')
- new_first: float32 [256, 512], P('fs', 'tp')
- new_second: float32 [256, 512], P('fs', 'tp')
All inputs are finite; a program needn't handle non-finite values.
Results may differ from a plain program's by a relative error of at most 0.006.
Values may be sent and summed in bfloat16 or wider, within the bound.
No kernel may reach another device: no remote copies, remote signals or barrier semaphores. Data moves between devices by JAX's collectives and lax.ppermute only.
A program may use at most 64 MiB of HBM per device.

v0:
```python
import jax
import jax.numpy as jnp
from jax import lax
from jax.sharding import PartitionSpec as P

RANK = 256
KW = 512


by_rows = (((0,), (0,)), ((), ()))


def sent_to_all(value, axis):
    count = lax.axis_size(axis)
    return lax.all_to_all(
        jnp.broadcast_to(value[None], (count, *value.shape)), axis, 0, 0, tiled=True
    )


def joined_along(tiles, dim):
    tiles = jnp.moveaxis(tiles, 0, dim)
    lengths = tiles.shape
    return tiles.reshape(*lengths[:dim], lengths[dim] * lengths[dim + 1], *lengths[dim + 2 :])


def gathered_copies(value, axis, dim):
    tiles = sent_to_all(value, axis)
    return joined_along(tiles, dim)


def cut_along(value, dim, count):
    lengths = value.shape
    tiles = value.reshape(*lengths[:dim], count, lengths[dim] // count, *lengths[dim + 1 :])
    return jnp.moveaxis(tiles, dim, 0)


def summed_on_arrival(value, axis, dim):
    count = lax.axis_size(axis)
    tiles = lax.all_to_all(cut_along(value, dim, count), axis, 0, 0, tiled=True)
    return jnp.sum(tiles, axis=0)


def over_copies(value, axis):
    return sent_to_all(value, axis).sum(axis=0)


def total_of_pieces(value, axis):
    return lax.all_gather(value, axis).sum(0)


def key_gradient(query_rows, key_rows, value_rows, grad_rows, second_scale):
    length = query_rows.shape[0]
    head_count = second_scale.shape[0]
    queries = query_rows.reshape(length, head_count, -1)
    keys_all = key_rows.reshape(length, head_count, -1)
    value_heads = value_rows.reshape(length, head_count, -1)
    grad_heads = grad_rows.reshape(length, head_count, -1)
    inv_root = queries.shape[2] ** (-0.5)
    scores = (
        jnp.einsum("qhd,khd->hqk", queries, keys_all, preferred_element_type=jnp.float32) * inv_root
    )
    positions = jnp.arange(length, dtype=jnp.int32)
    causal = positions[:, None] >= positions[None, :]
    scores = jnp.where(causal[None], scores, -1e30)
    row_peak = jnp.max(scores, axis=-1, keepdims=True)
    exps = jnp.exp(scores - row_peak)
    weights_map = exps / jnp.sum(exps, axis=-1, keepdims=True)
    attn_grad = jnp.einsum(
        "qhe,khe->hqk", grad_heads, value_heads, preferred_element_type=jnp.float32
    )
    row_inner = jnp.sum(weights_map * attn_grad, axis=-1, keepdims=True)
    score_grad = ((-second_scale)[:, None, None] * weights_map * (attn_grad - row_inner)).astype(
        jnp.bfloat16
    )
    key_grad = (
        jnp.einsum("hqk,qhd->khd", score_grad, queries, preferred_element_type=jnp.float32)
        * inv_root
    )
    return key_grad.reshape(length, -1).astype(jnp.bfloat16)


def on_device(
    tokens_in,
    query_two,
    key_two,
    values,
    out_grad,
    second_scale,
    factor,
    weight,
    first_moment,
    second_moment,
):
    key_grad = key_gradient(query_two, key_two, values, out_grad, second_scale)
    reduced = jnp.dot(
        tokens_in, gathered_copies(factor, "fs", 0), preferred_element_type=jnp.float32
    )
    reduced_high = reduced.astype(jnp.bfloat16)
    reduced_low = (reduced - reduced_high.astype(jnp.float32)).astype(jnp.bfloat16)
    first_part = lax.dot_general(
        reduced_high, key_grad, by_rows, preferred_element_type=jnp.float32
    )
    proj_part = summed_on_arrival(
        first_part
        + lax.dot_general(reduced_low, key_grad, by_rows, preferred_element_type=jnp.float32),
        "fs",
        0,
    )
    projected = over_copies(proj_part, "rep")
    new_first = 0.9 * first_moment + 0.1 * projected
    new_second = 0.95 * second_moment + 0.05 * projected * projected
    direction = (new_first / (jnp.sqrt(new_second) + 1e-08)).astype(jnp.bfloat16)
    gathered = gathered_copies(direction, "fs", 0)
    squares = total_of_pieces(jnp.sum(jnp.square(gathered.astype(jnp.float32))), "tp")
    update_step = jnp.dot(factor, gathered, preferred_element_type=jnp.float32) * lax.rsqrt(
        squares / (RANK * KW) + 1e-06
    )
    new_weight = weight - 0.1 * update_step
    copies = gathered_copies(new_weight.astype(jnp.bfloat16), "fs", 0)
    return (new_weight, copies, update_step, new_first, new_second)


def solution(mesh):
    in_specs = (
        P(("fs", "rep"), None),
        P(("fs", "rep"), "tp"),
        P(("fs", "rep"), "tp"),
        P(("fs", "rep"), "tp"),
        P(("fs", "rep"), "tp"),
        P("tp"),
        P("fs", None),
        P("fs", "tp"),
        P("fs", "tp"),
        P("fs", "tp"),
    )
    out_specs = (P("fs", "tp"), P(None, "tp"), P("fs", "tp"), P("fs", "tp"), P("fs", "tp"))
    return jax.shard_map(
        on_device, mesh=mesh, in_specs=in_specs, out_specs=out_specs, check_vma=False
    )
```

profile of v0, /device:TPU:8, one launch (start us, length us, event | category | flops | bytes accessed | tf_op | source)
XLA Modules:
  0.0 140.4 jit_solution(14205473987163703930)
XLA Ops:
  0.6 0.0 copy-start
  0.6 0.0 copy-start.6
  0.7 2.0 %broadcast_in_dim.20 = bf16[64,32,256]{2,1,0:T(8,128)(2,1)} broadcast(bf16[32,256]{1,0:T(8,128)(2,1)} %param.16), dimensions={1,2} | broadcast | bytes 1064960 | tf_op jit(solution)/shard_map/broadcast_in_dim | solution.py:16
  2.6 16.6 %all-to-all-start = ((bf16[64,32,256]{2,1,0:T(8,128)(2,1)}), bf16[64,32,256]{2,1,0:T(8,128)(2,1)S(1)}, u32[]{:S(2)}, u32[]{:S(2)}) async-start(bf16[64,32,256]{2,1,0:T(8,128)(2,1)} %broadcast_in_dim.20), calls=%async_computation | async-start | bytes 2097152 | tf_op jit(solution)/shard_map/all_to_all | solution.py:15
  19.2 1.1 copy.43
  20.3 0.0 copy-start.1
  20.3 1.9 %copy.44 = bf16[512,256]{0,1:T(8,128)(2,1)} copy(bf16[512,256]{1,0:T(8,128)(2,1)} %param.12) | data formatting | bytes 524288 | tf_op args[2]
  22.2 0.0 copy-done.6
  22.2 0.8 iota_compare_fusion
  23.0 3.8 %fusion.13 = f32[4,512,512]{1,2,0:T(8,128)} fusion(bf16[512,512]{1,0:T(8,128)(2,1)} %param.13, bf16[512,512]{1,0:T(8,128)(2,1)} %param.14), kind=kOutput, calls=%fused_computation.20 | convolution fusion | flops 268435456 | bytes 5242880 | tf_op jit(solution)/shard_map/qhe,khe->hqk/dot_general | solution.py:68
  26.9 6.8 %multiply_reduce_fusion = (f32[4,512]{1,0:T(4,128)S(1)}, f32[4,512,512]{1,2,0:T(8,128)}) fusion(f32[4,512,512]{1,2,0:T(8,128)} %fusion.13, pred[512,512]{0,1:T(8,128)(4,1)} %iota_compare_fusion, bf16[512,4,64]{0,2,1:T(8,128)(2,1)S(1)} %bitcast.40, bf16[512,4,64]{0,2,1:T(8,128)(2,1)} %bitcast.42), kind=kOutput, calls=%fused_computation.3 | convolution fusion | flops 140512256 | bytes 9183232 | tf_op jit(solution)/shard_map/div | solution.py:67
  33.7 0.0 copy-done.1
  33.7 4.3 %fusion.11 = bf16[4,512,64]{1,2,0:T(8,128)(2,1)S(1)} fusion(bf16[512,4,64]{0,2,1:T(8,128)(2,1)} %bitcast.41, f32[4,512,512]{1,2,0:T(8,128)} %fusion.13, f32[4,512,512]{1,2,0:T(8,128)} %get-tuple-element.11, f32[4,512]{1,0:T(4,128)S(1)} %get-tuple-element.10, f32[4]{0:T(128)S(1)} %neg.3), kind=kOutput, calls=%fused_computation.15 | convolution fusion | flops 138674176 | bytes 8921104 | tf_op jit(solution)/shard_map/hqk,qhd->khd/dot_general | solution.py:76
  38.0 0.0 copy-start.4
  38.0 0.0 copy-start.5
  38.0 10.5 %all-to-all-done = bf16[64,32,256]{2,1,0:T(8,128)(2,1)S(1)} async-done(((bf16[64,32,256]{2,1,0:T(8,128)(2,1)}), bf16[64,32,256]{2,1,0:T(8,128)(2,1)S(1)}, u32[]{:S(2)}, u32[]{:S(2)}) %all-to-all-start) | async-done | bytes 1048608 | tf_op jit(solution)/shard_map/all_to_all | solution.py:15
  48.5 0.0 copy-done
  48.5 0.0 copy-start.2
  48.5 0.0 copy-start.3
  48.5 0.7 fusion.31
  49.2 0.3 fusion.21
  49.5 0.3 convolution_add_fusion
  49.8 0.1 reshape.61
  49.9 20.2 %all_to_all.25 = f32[64,4,256]{2,1,0:T(4,128)S(1)} all-to-all(f32[64,4,256]{2,1,0:T(4,128)S(1)} %reshape.61), channel_id=1, replica_groups=mesh['fs'=64,'rep'=4,'tp'=2] {'fs'}, dimensions={0} | all-to-all | bytes 524288 | tf_op jit(solution)/shard_map/all_to_all | solution.py:39
  70.0 0.1 reduce_sum.56
  70.1 9.4 %all_to_all.26 = f32[4,4,256]{2,1,0:T(4,128)S(1)} all-to-all(f32[4,4,256]{2,1,0:T(4,128)S(1)} %broadcast_in_dim.23), channel_id=1, replica_groups=mesh['fs'=64,'rep'=4,'tp'=2] {'rep'}, dimensions={0} | all-to-all | bytes 32768 | tf_op jit(solution)/shard_map/all_to_all | solution.py:15
  79.6 0.0 copy-done.4
  79.6 0.0 copy-done.5
  79.6 0.6 fusion.24
  80.2 0.7 broadcast_in_dim.24
  80.9 5.1 %all-to-all-start.3 = ((bf16[64,4,256]{2,1,0:T(4,128)(2,1)}), bf16[64,4,256]{2,1,0:T(4,128)(2,1)S(1)}, u32[]{:S(2)}, u32[]{:S(2)}) async-start(bf16[64,4,256]{2,1,0:T(4,128)(2,1)} %broadcast_in_dim.24), calls=%async_computation.3 | async-start | bytes 262144 | tf_op jit(solution)/shard_map/all_to_all | solution.py:15
  86.1 1.3 dynamic-slice
  87.3 10.7 %all-to-all-done.3 = bf16[64,4,256]{2,1,0:T(4,128)(2,1)S(1)} async-done(((bf16[64,4,256]{2,1,0:T(4,128)(2,1)}), bf16[64,4,256]{2,1,0:T(4,128)(2,1)S(1)}, u32[]{:S(2)}, u32[]{:S(2)}) %all-to-all-start.3) | async-done | bytes 131104 | tf_op jit(solution)/shard_map/all_to_all | solution.py:15
  98.1 0.7 multiply_reduce_fusion.1
  98.8 1.4 dynamic-update-slice
  100.2 2.4 %all-reduce = f32[2]{0:T(128)S(1)} all-reduce(f32[2]{0:T(128)S(1)} %dynamic-update-slice), channel_id=1, replica_groups=mesh['fs'=64,'rep'=4,'tp'=2] {'tp'}, use_global_device_ids=true, to_apply=%add | all-reduce | flops 2 | bytes 16
  102.6 0.6 reduce_sum.59
  103.9 0.0 copy-done.2
  103.9 0.0 copy-done.3
  104.0 0.8 fusion.27
  104.7 0.1 broadcast_in_dim.25
  104.9 34.6 %all_to_all.27 = bf16[64,32,256]{2,1,0:T(8,128)(2,1)S(1)} all-to-all(bf16[64,32,256]{2,1,0:T(8,128)(2,1)S(1)} %broadcast_in_dim.25), channel_id=1, replica_groups=mesh['fs'=64,'rep'=4,'tp'=2] {'fs'}, dimensions={0} | all-to-all | bytes 2097152 | tf_op jit(solution)/shard_map/all_to_all | solution.py:15
  139.4 1.0 copy.63
  (5 shorter events, 0.1 us)
Async XLA Ops:
  0.6 47.9 %copy-start = (bf16[512,2048]{1,0:T(8,128)(2,1)S(1)}, bf16[512,2048]{1,0:T(8,128)(2,1)}, u32[]{:S(2)}) copy-start(bf16[512,2048]{1,0:T(8,128)(2,1)} %param.10) | copy-start | bytes 6291460
  0.6 21.6 %copy-start.6 = (f32[4]{0:T(128)S(1)}, f32[4]{0:T(128)}, u32[]{:S(2)}) copy-start(f32[4]{0:T(128)} %param.15) | copy-start | bytes 52
  2.6 45.9 %all-to-all-start = ((bf16[64,32,256]{2,1,0:T(8,128)(2,1)}), bf16[64,32,256]{2,1,0:T(8,128)(2,1)S(1)}, u32[]{:S(2)}, u32[]{:S(2)}) async-start(bf16[64,32,256]{2,1,0:T(8,128)(2,1)} %broadcast_in_dim.20), calls=%async_computation | async-start | bytes 2097152 | tf_op jit(solution)/shard_map/all_to_all | solution.py:15
  20.3 13.4 %copy-start.1 = (bf16[512,256]{0,1:T(8,128)(2,1)}, bf16[512,256]{0,1:T(8,128)(2,1)S(1)}, u32[]{:S(2)}) copy-start(bf16[512,256]{0,1:T(8,128)(2,1)S(1)} %copy.43) | copy-start | bytes 786436
  38.0 41.6 %copy-start.4 = (f32[4,256]{1,0:T(4,128)S(1)}, f32[4,256]{1,0:T(4,128)}, u32[]{:S(2)}) copy-start(f32[4,256]{1,0:T(4,128)} %param.19) | copy-start | bytes 12292
  38.0 41.6 %copy-start.5 = (f32[4,256]{1,0:T(4,128)S(1)}, f32[4,256]{1,0:T(4,128)}, u32[]{:S(2)}) copy-start(f32[4,256]{1,0:T(4,128)} %param.18) | copy-start | bytes 12292
  48.5 55.4 %copy-start.2 = (bf16[32,256]{1,0:T(8,128)(2,1)S(1)}, bf16[32,256]{1,0:T(8,128)(2,1)}, u32[]{:S(2)}) copy-start(bf16[32,256]{1,0:T(8,128)(2,1)} %param.16) | copy-start | bytes 49156
  48.5 55.4 %copy-start.3 = (f32[32,256]{1,0:T(8,128)S(1)}, f32[32,256]{1,0:T(8,128)}, u32[]{:S(2)}) copy-start(f32[32,256]{1,0:T(8,128)} %param.17) | copy-start | bytes 98308
  80.9 17.2 %all-to-all-start.3 = ((bf16[64,4,256]{2,1,0:T(4,128)(2,1)}), bf16[64,4,256]{2,1,0:T(4,128)(2,1)S(1)}, u32[]{:S(2)}, u32[]{:S(2)}) async-start(bf16[64,4,256]{2,1,0:T(4,128)(2,1)} %broadcast_in_dim.24), calls=%async_computation.3 | async-start | bytes 262144 | tf_op jit(solution)/shard_map/all_to_all | solution.py:15
where the time goes:
time: 141 us; the launch traced here: 140 us
  blocking collectives  66.6 us (47%)
  starting transfers between devices  21.7 us (15%)
  waiting for transfers between devices  21.3 us (15%)
  matrix products  17 us (12%)
  local copies, waits for them, and re-layouts  9.58 us (7%)
  other arithmetic  2.76 us (2%)
  between operations  1.48 us (1%)
    all_to_all x2, blocking collectives, sent_to_all(): lax.all_to_all(jnp.broadcast_to(value[None], (count, *value.shape)), axis...  44 us
    all_to_all x2, starting transfers between devices, sent_to_all(): lax.all_to_all(jnp.broadcast_to(value[None], (count, *value.shape)), axis...  21.7 us
    all_to_all x2, waiting for transfers between devices, sent_to_all(): lax.all_to_all(jnp.broadcast_to(value[None], (count, *value.shape)), axis...  21.3 us
    all_to_all x1, blocking collectives, summed_on_arrival(): tiles = lax.all_to_all(cut_along(value, dim, count), axis, 0, 0, tiled=True)  20.2 us
    div x1, matrix products, key_gradient(): weights_map = exps / jnp.sum(exps, axis=-1, keepdims=True)  6.81 us
    unnamed x20, local copies, waits for them, and re-layouts  6.68 us
    dot_general x1, matrix products, key_gradient(): jnp.einsum('hqk,qhd->khd', score_grad, queries, preferred_element_type=jn...  4.29 us
    dot_general x1, matrix products, key_gradient(): jnp.einsum('qhe,khe->hqk', grad_heads, value_heads, preferred_element_typ...  3.83 us
  transfers between devices with their start and end apart: 2, of which 2 were waited for; matrix products, arithmetic and copies ran while one was open for 14% of the time, Pallas kernels for 0%

commit v1 on v0

v1 whole, which is shorter than its diff:
```python
import jax
import jax.numpy as jnp
from jax import lax
from jax.sharding import PartitionSpec as P


RANK = 256
KW = 512
BF16 = jnp.bfloat16
F32 = jnp.float32

by_rows = (((0,), (0,)), ((), ()))


def dot32(left, right):
    return jnp.dot(left, right, preferred_element_type=F32)


def sent_to_all(value, axis, count):
    return lax.all_to_all(
        jnp.broadcast_to(value[None], (count, *value.shape)), axis, 0, 0, tiled=True
    )


def to_bf16(value):
    return lax.reduce_precision(value, exponent_bits=8, mantissa_bits=7)


def parts_of(value):
    high = to_bf16(value)
    middle = to_bf16(value - high)
    low = to_bf16(value - high - middle)
    return high.astype(BF16), middle.astype(BF16), low.astype(BF16)


def key_gradient(query_rows, key_rows, value_rows, grad_rows, second_scale):
    length = query_rows.shape[0]
    head_count = second_scale.shape[0]
    queries = query_rows.reshape(length, head_count, -1)
    keys_all = key_rows.reshape(length, head_count, -1)
    value_heads = value_rows.reshape(length, head_count, -1)
    grad_heads = grad_rows.reshape(length, head_count, -1)
    inv_root = queries.shape[2] ** (-0.5)
    scores = (
        jnp.einsum("qhd,khd->hqk", queries, keys_all, preferred_element_type=jnp.float32) * inv_root
    )
    positions = jnp.arange(length, dtype=jnp.int32)
    causal = positions[:, None] >= positions[None, :]
    scores = jnp.where(causal[None], scores, -1e30)
    row_peak = jnp.max(scores, axis=-1, keepdims=True)
    exps = jnp.exp(scores - row_peak)
    weights_map = exps / jnp.sum(exps, axis=-1, keepdims=True)
    attn_grad = jnp.einsum(
        "qhe,khe->hqk", grad_heads, value_heads, preferred_element_type=jnp.float32
    )
    row_inner = jnp.sum(weights_map * attn_grad, axis=-1, keepdims=True)
    score_grad = ((-second_scale)[:, None, None] * weights_map * (attn_grad - row_inner)).astype(
        jnp.bfloat16
    )
    key_grad = (
        jnp.einsum("hqk,qhd->khd", score_grad, queries, preferred_element_type=jnp.float32)
        * inv_root
    )
    return key_grad.reshape(length, -1).astype(jnp.bfloat16)


def on_device(
    tokens_in,
    query_two,
    key_two,
    values,
    out_grad,
    second_scale,
    factor,
    weight,
    first_moment,
    second_moment,
):
    shards = lax.axis_size("fs")
    reps = lax.axis_size("rep")
    core = lax.axis_index("tp")
    rank = factor.shape[1]
    half = rank // 2
    own_rows = first_moment.shape[0]
    pairs = own_rows // 2
    rows_here, cols = weight.shape

    ranks = lax.broadcasted_iota(jnp.int32, (rank, half), 0)
    places = lax.broadcasted_iota(jnp.int32, (rank, half), 1)
    mine = dot32(factor, (ranks == 2 * places + core).astype(BF16)).astype(BF16)
    other = dot32(factor, (ranks == 2 * places + 1 - core).astype(BF16)).astype(BF16)

    share = rows_here // reps
    rep = lax.axis_index("rep")
    old_share = lax.dynamic_slice_in_dim(weight, rep * share, share, 0).astype(BF16)
    old_share = jnp.concatenate([old_share[:, i : i + half] for i in range(0, cols, half)], axis=0)
    first_sent = sent_to_all(jnp.concatenate([mine, old_share], axis=0), "fs", shards)
    factor_mine = first_sent[:, :rows_here].reshape(-1, half)
    old_mine = first_sent[:, rows_here:]

    moments = lax.all_gather(jnp.concatenate([first_moment, second_moment], 0), "tp")
    moments = jnp.concatenate([moments[0], moments[1]], axis=1)
    first_both, second_both = moments[:own_rows], moments[own_rows:]

    key_grad = key_gradient(query_two, key_two, values, out_grad, second_scale)
    key_both = lax.all_gather(key_grad, "tp")

    reduced = dot32(tokens_in, factor_mine)
    reduced_high = reduced.astype(BF16)
    reduced_low = (reduced - reduced_high.astype(F32)).astype(BF16)
    sums = [
        lax.dot_general(reduced_high, key_both[i], by_rows, preferred_element_type=F32)
        + lax.dot_general(reduced_low, key_both[i], by_rows, preferred_element_type=F32)
        for i in range(2)
    ]
    sums = jnp.concatenate(sums, axis=1).astype(BF16)

    arrived = lax.all_to_all(sums.reshape(shards, pairs, 2 * cols), "fs", 0, 0, tiled=True)
    factor_other = lax.ppermute(factor_mine, "tp", [(0, 1), (1, 0)])
    factor_all = jnp.concatenate([factor_mine, factor_other], axis=1)
    own_factor = jnp.concatenate([mine, other], axis=1)
    old_all = jnp.zeros((shards, reps, *old_mine.shape[1:]), BF16)
    old_all = lax.dynamic_update_index_in_dim(old_all, old_mine, rep, 1)
    for i in range(1, reps):
        came = lax.ppermute(old_mine, "rep", [(j, (j + i) % reps) for j in range(reps)])
        old_all = lax.dynamic_update_index_in_dim(old_all, came, (rep + reps - i) % reps, 1)
    old_all = old_all.reshape(shards, reps, cols // half, share, half)
    old_weight = jnp.moveaxis(old_all, 2, 3).reshape(-1, cols)

    part = jnp.sum(arrived.astype(F32), axis=0)
    part = sent_to_all(part, ("rep", "tp"), 2 * reps)
    part = part.reshape(reps, 2, pairs, 2 * cols).sum(axis=0)
    projected = jnp.stack([part[0], part[1]], axis=1).reshape(own_rows, 2 * cols)

    new_first = 0.9 * first_both + 0.1 * projected
    new_second = 0.95 * second_both + 0.05 * projected * projected
    direction = (new_first / (jnp.sqrt(new_second) + 1e-08)).astype(BF16)
    own_squares = jnp.sum(jnp.square(direction.astype(F32)))

    def own_cols(value):
        return jnp.where(core == 0, value[:, :cols], value[:, cols:])

    own_direction = own_cols(direction).reshape(pairs, 2 * cols)
    high, middle, low = parts_of(own_squares)
    lane = lax.broadcasted_iota(jnp.int32, (pairs, 128), 1)
    row = lax.broadcasted_iota(jnp.int32, (pairs, 128), 0)
    zero = jnp.zeros((), BF16)
    packed = jnp.where(lane == 0, high, jnp.where(lane == 1, middle, jnp.where(lane == 2, low, zero)))
    packed = jnp.where(row == 0, packed, zero)
    gathered = sent_to_all(jnp.concatenate([own_direction, packed], axis=1), "fs", shards)
    squares = jnp.sum(gathered[:, :, 2 * cols :].astype(F32))
    even = gathered[:, :, :cols].reshape(-1, cols)
    odd = gathered[:, :, cols : 2 * cols].reshape(-1, cols)
    rows = jnp.concatenate(
        [jnp.where(core == 0, even, odd), jnp.where(core == 0, odd, even)], axis=0
    )

    rate = lax.rsqrt(squares / (RANK * KW) + 1e-06)
    update_step = dot32(own_factor, rows) * rate
    new_weight = weight - 0.1 * update_step
    copies = (old_weight.astype(F32) - 0.1 * (dot32(factor_all, rows) * rate)).astype(BF16)
    return (new_weight, copies, update_step, own_cols(new_first), own_cols(new_second))


def solution(mesh):
    in_specs = (
        P(("fs", "rep"), None),
        P(("fs", "rep"), "tp"),
        P(("fs", "rep"), "tp"),
        P(("fs", "rep"), "tp"),
        P(("fs", "rep"), "tp"),
        P("tp"),
        P("fs", None),
        P("fs", "tp"),
        P("fs", "tp"),
        P("fs", "tp"),
    )
    out_specs = (P("fs", "tp"), P(None, "tp"), P("fs", "tp"), P("fs", "tp"), P("fs", "tp"))

    return jax.shard_map(
        on_device, mesh=mesh, in_specs=in_specs, out_specs=out_specs, check_vma=False
    )
```

time: 141 us -> 127 us (0.901)
  blocking collectives: 66.6 us -> 3.99 us
  starting transfers between devices: 21.7 us -> 58 us
  waiting for transfers between devices: 21.3 us -> 13.7 us
  between operations: 1.48 us -> 7.22 us
  other arithmetic: 2.76 us -> 8.27 us
  matrix products: 17 us -> 21.4 us
  local copies, waits for them, and re-layouts: 9.58 us -> 13.2 us
    all_to_all x3 -> x0, blocking collectives: 64.2 us -> none  [the longest x2 44 us: sent_to_all(): lax.all_to_all(jnp.broadcast_to(value[None], (count, *value.shape)), axis...]
    ppermute x0 -> x4, starting transfers between devices: none -> 13.3 us  [the longest x3 11.4 us: on_device(): lax.ppermute(old_mine, 'rep', [(j, (j + i) % reps) for j in range(reps)])]
    all_to_all x0 -> x1, starting transfers between devices: none -> 11.9 us  [on_device(): lax.all_to_all(sums.reshape(shards, pairs, 2 * cols), 'fs', 0, 0, tiled=T...]
    all_to_all x2 -> x3, starting transfers between devices: 21.7 us -> 32.8 us  [sent_to_all(): lax.all_to_all(jnp.broadcast_to(value[None], (count, *value.shape)), axis...]
    all_to_all x2 -> x3, waiting for transfers between devices: 21.3 us -> 13.7 us  [sent_to_all(): lax.all_to_all(jnp.broadcast_to(value[None], (count, *value.shape)), axis...]
    dot_general x4 -> x9, matrix products: 2.04 us -> 6.64 us  [the longest x5 5.88 us: dot32(): return jnp.dot(left, right, preferred_element_type=F32)]
    unnamed x20 -> x27, local copies, waits for them, and re-layouts: 6.68 us -> 2.25 us
    slice x0 -> x5, local copies, waits for them, and re-layouts: none -> 4.18 us  [the longest x1 1.87 us: on_device(): factor_mine = first_sent[:, :rows_here].reshape(-1, half)]
  transfers between devices with their start and end apart: 2 -> 8, of which waited for: 2 -> 3; matrix products, arithmetic and copies ran while one was open for 14% -> 25% of each run, Pallas kernels for 0% -> 0%
where the time goes in v1:
time: 127 us; the launch traced here: 126 us
  starting transfers between devices  58 us (46%)
  matrix products  21.4 us (17%)
  waiting for transfers between devices  13.7 us (11%)
  local copies, waits for them, and re-layouts  13.2 us (10%)
  other arithmetic  8.27 us (7%)
  between operations  7.22 us (6%)
  blocking collectives  3.99 us (3%)
    all_to_all x3, starting transfers between devices, sent_to_all(): lax.all_to_all(jnp.broadcast_to(value[None], (count, *value.shape)), axis...  32.8 us
    all_to_all x3, waiting for transfers between devices, sent_to_all(): lax.all_to_all(jnp.broadcast_to(value[None], (count, *value.shape)), axis...  13.7 us
    all_to_all x1, starting transfers between devices, on_device(): lax.all_to_all(sums.reshape(shards, pairs, 2 * cols), 'fs', 0, 0, tiled=T...  11.9 us
    ppermute x3, starting transfers between devices, on_device(): lax.ppermute(old_mine, 'rep', [(j, (j + i) % reps) for j in range(reps)])  11.4 us
    div x1, matrix products, key_gradient(): weights_map = exps / jnp.sum(exps, axis=-1, keepdims=True)  6.64 us
    dot_general x5, matrix products, dot32(): return jnp.dot(left, right, preferred_element_type=F32)  5.88 us
    dot_general x1, matrix products, key_gradient(): jnp.einsum('hqk,qhd->khd', score_grad, queries, preferred_element_type=jn...  4.3 us
    dot_general x1, matrix products, key_gradient(): jnp.einsum('qhe,khe->hqk', grad_heads, value_heads, preferred_element_typ...  3.86 us
  transfers between devices with their start and end apart: 8, of which 3 were waited for; matrix products, arithmetic and copies ran while one was open for 25% of the time, Pallas kernels for 0%

profile of v1, /device:TPU:8, one launch (start us, length us, event | category | flops | bytes accessed | tf_op | source)
XLA Modules:
  0.0 125.9 jit_solution(13278281564107936511)
XLA Ops:
  0.7 0.8 dynamic-slice_convert_fusion
  1.5 0.9 fusion.15
  2.4 1.0 broadcast_in_dim.72
  3.4 16.7 %all-to-all-start = ((bf16[64,48,128]{2,1,0:T(8,128)(2,1)}), bf16[64,48,128]{2,1,0:T(8,128)(2,1)}, u32[]{:S(2)}, u32[]{:S(2)}) async-start(bf16[64,48,128]{2,1,0:T(8,128)(2,1)} %broadcast_in_dim.72), calls=%async_computation | async-start | bytes 1572864 | tf_op jit(solution)/shard_map/all_to_all | solution.py:20
  20.2 1.1 copy.75
  21.3 1.1 copy.76
  22.4 3.9 %fusion.20 = f32[4,512,512]{1,2,0:T(8,128)} fusion(bf16[512,512]{1,0:T(8,128)(2,1)} %param.13, bf16[512,512]{1,0:T(8,128)(2,1)} %param.14), kind=kOutput, calls=%fused_computation.34 | convolution fusion | flops 268435456 | bytes 5242880 | tf_op jit(solution)/shard_map/qhe,khe->hqk/dot_general | solution.py:53
  26.3 6.6 %multiply_reduce_fusion = (f32[4,512]{1,0:T(4,128)S(1)}, f32[4,512,512]{1,2,0:T(8,128)}) fusion(f32[4,512,512]{1,2,0:T(8,128)} %fusion.20, pred[512,512]{0,1:T(8,128)(4,1)S(1)} %iota_compare_fusion, bf16[512,4,64]{0,2,1:T(8,128)(2,1)S(1)} %bitcast.71, bf16[512,4,64]{0,2,1:T(8,128)(2,1)S(1)} %bitcast.74), kind=kOutput, calls=%fused_computation.3 | convolution fusion | flops 140512256 | bytes 9183232 | tf_op jit(solution)/shard_map/div | solution.py:52
  32.9 4.3 %fusion.12 = bf16[4,512,64]{1,2,0:T(8,128)(2,1)S(1)} fusion(bf16[512,4,64]{0,2,1:T(8,128)(2,1)S(1)} %bitcast.72, f32[4,512,512]{1,2,0:T(8,128)} %fusion.20, f32[4,512,512]{1,2,0:T(8,128)} %get-tuple-element.18, f32[4,512]{1,0:T(4,128)S(1)} %get-tuple-element.17, f32[4]{0:T(128)S(1)} %neg.3), kind=kOutput, calls=%fused_computation.18 | convolution fusion | flops 138674176 | bytes 8921104 | tf_op jit(solution)/shard_map/hqk,qhd->khd/dot_general | solution.py:61
  37.4 1.8 %all-gather = f32[16,256]{1,0:T(8,128)S(1)} all-gather(f32[8,256]{1,0:T(8,128)S(1)} %pad_maximum_fusion.3), channel_id=2, replica_groups=mesh['fs'=64,'rep'=4,'tp'=2] {'tp'}, dimensions={0}, use_global_device_ids=true | all-gather | bytes 24576 | tf_op jit(solution)/shard_map/all_gather | solution.py:101
  39.3 0.5 iota_compare_fusion.5
  39.8 2.2 %all_gather.12 = bf16[2,512,256]{2,1,0:T(8,128)(2,1)S(1)} all-gather(bf16[1,512,256]{2,1,0:T(8,128)(2,1)S(1)} %copy.80), channel_id=1, replica_groups=mesh['fs'=64,'rep'=4,'tp'=2] {'tp'}, dimensions={0}, use_global_device_ids=true | all-gather | bytes 786432 | tf_op jit(solution)/shard_map/all_gather | solution.py:106
  41.9 0.6 fusion.50
  42.5 0.7 fusion.16
  43.3 0.8 all-to-all-done
  44.0 1.9 %slice.94 = bf16[64,32,128]{2,1,0:T(8,128)(2,1)} slice(bf16[64,48,128]{2,1,0:T(8,128)(2,1)} %all-to-all-done), slice={[0:64], [0:32], [0:128]} | slice | bytes 1048576 | tf_op jit(solution)/shard_map/slice | solution.py:98
  45.9 1.9 %convolution_bitcast_fusion = f32[512,128]{0,1:T(8,128)S(1)} fusion(bf16[2048,128]{1,0:T(8,128)(2,1)} %bitcast.2, bf16[512,2048]{1,0:T(8,128)(2,1)S(1)} %copy-done), kind=kOutput, calls=%fused_computation.19 | convolution fusion | flops 268435456 | bytes 2883584 | tf_op jit(solution)/shard_map/dot_general | solution.py:16
  47.8 0.2 fusion.28
  48.0 0.2 fusion.27
  48.2 0.2 fusion.14
  48.4 0.2 fusion.13
  48.6 0.8 pad_maximum_fusion
  49.4 11.9 %all-to-all-start.1 = ((bf16[64,2,512]{2,1,0:T(2,128)(2,1)}), bf16[64,2,512]{2,1,0:T(2,128)(2,1)S(1)}, u32[]{:S(2)}, u32[]{:S(2)}) async-start(bf16[64,2,512]{2,1,0:T(2,128)(2,1)} %pad_maximum_fusion), calls=%async_computation.1 | async-start | bytes 262144 | tf_op jit(solution)/shard_map/all_to_all | solution.py:118
  61.4 0.5 iota_compare_fusion.7
  61.9 1.7 %slice.104 = bf16[64,16,128]{2,1,0:T(8,128)(2,1)} slice(bf16[64,48,128]{2,1,0:T(8,128)(2,1)} %all-to-all-done), slice={[0:64], [32:48], [0:128]} | slice | bytes 524288 | tf_op jit(solution)/shard_map/slice | solution.py:99
  63.6 3.4 %collective-permute-start = (bf16[64,16,128]{2,1,0:T(8,128)(2,1)}, bf16[64,16,128]{2,1,0:T(8,128)(2,1)}, u32[]{:S(2)}, u32[]{:S(2)}) collective-permute-start(bf16[64,16,128]{2,1,0:T(8,128)(2,1)} %slice.104), channel_id=1, source_target_pairs={{0,2},{2,4},{4,6},{6,0},{1,3},{3,5},{5,7},{7,1},{8,10},{10,12},{12... | collective-permute-start | bytes 786440 | tf_op jit(solution)/shard_map/ppermute | solution.py:125
  67.0 4.6 %collective-permute-start.1 = (bf16[64,16,128]{2,1,0:T(8,128)(2,1)}, bf16[64,16,128]{2,1,0:T(8,128)(2,1)}, u32[]{:S(2)}, u32[]{:S(2)}) collective-permute-start(bf16[64,16,128]{2,1,0:T(8,128)(2,1)} %slice.104), channel_id=1, source_target_pairs={{0,4},{2,6},{4,0},{6,2},{1,5},{3,7},{5,1},{7,3},{8,12},{10,14},{12... | collective-permute-start | bytes 786440 | tf_op jit(solution)/shard_map/ppermute | solution.py:125
  71.6 3.3 %collective-permute-start.2 = (bf16[64,16,128]{2,1,0:T(8,128)(2,1)}, bf16[64,16,128]{2,1,0:T(8,128)(2,1)S(1)}, u32[]{:S(2)}, u32[]{:S(2)}) collective-permute-start(bf16[64,16,128]{2,1,0:T(8,128)(2,1)} %slice.104), channel_id=1, source_target_pairs={{0,6},{2,0},{4,2},{6,4},{1,7},{3,1},{5,3},{7,5},{8,14},{10,8},{12,... | collective-permute-start | bytes 786440 | tf_op jit(solution)/shard_map/ppermute | solution.py:125
  75.0 1.9 %collective-permute-start.3 = (bf16[2048,128]{1,0:T(8,128)(2,1)}, bf16[2048,128]{1,0:T(8,128)(2,1)}, u32[]{:S(2)}, u32[]{:S(2)}) collective-permute-start(bf16[2048,128]{1,0:T(8,128)(2,1)} %bitcast.2), channel_id=1, source_target_pairs={{0,1},{1,0},{2,3},{3,2},{4,5},{5,4},{6,7},{7,6},{8,9},{9,8},{10,11... | collective-permute-start | bytes 1572872 | tf_op jit(solution)/shard_map/ppermute | solution.py:119
  76.9 0.2 broadcast_in_dim.82
  77.2 1.0 bitcast_dynamic-update-slice_fusion.2
  78.4 0.6 broadcast_in_dim.75
  79.0 3.3 %all-to-all-start.2 = ((f32[8,2,512]{2,1,0:T(2,128)}), f32[8,2,512]{2,1,0:T(2,128)S(1)}, u32[]{:S(2)}, u32[]{:S(2)}) async-start(f32[8,2,512]{2,1,0:T(2,128)} %broadcast_in_dim.75), calls=%async_computation.2 | async-start | bytes 65536 | tf_op jit(solution)/shard_map/all_to_all | solution.py:20
  82.4 1.0 bitcast_dynamic-update-slice_fusion.1
  83.4 1.0 bitcast_dynamic-update-slice_fusion
  84.4 1.6 %bitcast_convert_fusion = f32[64,4,2,8,128]{4,3,2,1,0:T(8,128)} fusion(bf16[64,4,16,128]{3,2,1,0:T(8,128)(2,1)S(1)} %bitcast_dynamic-update-slice_fusion.3), kind=kLoop, calls=%fused_computation.32 | loop fusion | flops 524288 | bytes 3145728 | tf_op jit(solution)/shard_map/convert_element_type | solution.py:161
  86.0 1.7 %all-to-all-done.2 = f32[8,2,512]{2,1,0:T(2,128)S(1)} async-done(((f32[8,2,512]{2,1,0:T(2,128)}), f32[8,2,512]{2,1,0:T(2,128)S(1)}, u32[]{:S(2)}, u32[]{:S(2)}) %all-to-all-start.2) | async-done | bytes 32800 | tf_op jit(solution)/shard_map/all_to_all | solution.py:20
  87.8 0.6 multiply_reduce_fusion.1
  93.9 0.6 compare_select_fusion
  94.7 0.8 broadcast_in_dim.81
  95.4 12.7 %all-to-all-start.3 = ((bf16[64,2,640]{2,1,0:T(2,128)(2,1)}), bf16[64,2,640]{2,1,0:T(2,128)(2,1)S(1)}, u32[]{:S(2)}, u32[]{:S(2)}) async-start(bf16[64,2,640]{2,1,0:T(2,128)(2,1)} %broadcast_in_dim.81), calls=%async_computation.3 | async-start | bytes 327680 | tf_op jit(solution)/shard_map/all_to_all | solution.py:20
  108.1 0.6 slice_select_fusion.1
  108.7 0.6 slice_select_fusion
  109.3 11.2 %all-to-all-done.3 = bf16[64,2,640]{2,1,0:T(2,128)(2,1)S(1)} async-done(((bf16[64,2,640]{2,1,0:T(2,128)(2,1)}), bf16[64,2,640]{2,1,0:T(2,128)(2,1)S(1)}, u32[]{:S(2)}, u32[]{:S(2)}) %all-to-all-start.3) | async-done | bytes 163872 | tf_op jit(solution)/shard_map/all_to_all | solution.py:20
  120.7 0.6 convert_reduce_fusion.1
  122.1 0.8 multiply_subtract_fusion
  122.9 1.6 %fusion.3 = f32[2048,256]{1,0:T(8,128)S(1)} fusion(bf16[256,256]{1,0:T(8,128)(2,1)S(1)} %constant_dynamic-update-slice_fusion, bf16[2048,128]{1,0:T(8,128)(2,1)} %collective-permute-done.3, bf16[2048,128]{1,0:T(8,128)(2,1)} %bitcast.2, f32[]{:T(128)S(6)} %rsqrt.3), kind=kOutput, calls=%fused_computation.8 | convolution fusion | flops 271581184 | bytes 3276804 | tf_op jit(solution)/shard_map/dot_general | solution.py:16
  124.6 1.3 %subtract_convert_fusion = bf16[2048,256]{1,0:T(8,128)(2,1)} fusion(f32[2048,256]{1,0:T(8,128)S(1)} %bitcast.70, f32[2048,256]{1,0:T(8,128)S(1)} %fusion.3), kind=kLoop, calls=%fused_computation.11 | loop fusion | flops 1048576 | bytes 5242880 | tf_op jit(solution)/shard_map/convert_element_type | solution.py:161
  (55 shorter events, 1.0 us)
Async XLA Ops:
  0.6 45.3 %copy-start = (bf16[512,2048]{1,0:T(8,128)(2,1)S(1)}, bf16[512,2048]{1,0:T(8,128)(2,1)}, u32[]{:S(2)}) copy-start(bf16[512,2048]{1,0:T(8,128)(2,1)} %param.10) | copy-start | bytes 6291460
  3.4 40.7 %all-to-all-start = ((bf16[64,48,128]{2,1,0:T(8,128)(2,1)}), bf16[64,48,128]{2,1,0:T(8,128)(2,1)}, u32[]{:S(2)}, u32[]{:S(2)}) async-start(bf16[64,48,128]{2,1,0:T(8,128)(2,1)} %broadcast_in_dim.72), calls=%async_computation | async-start | bytes 1572864 | tf_op jit(solution)/shard_map/all_to_all | solution.py:20
  26.3 6.6 %copy-start.11 = (f32[4]{0:T(128)S(1)}, f32[4]{0:T(128)}, u32[]{:S(2)}) copy-start(f32[4]{0:T(128)} %param.15) | copy-start | bytes 52
  32.9 4.5 %copy-start.5 = (f32[4,256]{1,0:T(4,128)S(1)}, f32[4,256]{1,0:T(4,128)}, u32[]{:S(2)}) copy-start(f32[4,256]{1,0:T(4,128)} %param.19) | copy-start | bytes 12292
  32.9 4.5 %copy-start.6 = (f32[4,256]{1,0:T(4,128)S(1)}, f32[4,256]{1,0:T(4,128)}, u32[]{:S(2)}) copy-start(f32[4,256]{1,0:T(4,128)} %param.18) | copy-start | bytes 12292
  32.9 9.6 %copy-start.10 = (bf16[32,256]{1,0:T(8,128)(2,1)S(1)}, bf16[32,256]{1,0:T(8,128)(2,1)}, u32[]{:S(2)}) copy-start(bf16[32,256]{1,0:T(8,128)(2,1)} %param.16) | copy-start | bytes 49156
  49.4 28.7 %all-to-all-start.1 = ((bf16[64,2,512]{2,1,0:T(2,128)(2,1)}), bf16[64,2,512]{2,1,0:T(2,128)(2,1)S(1)}, u32[]{:S(2)}, u32[]{:S(2)}) async-start(bf16[64,2,512]{2,1,0:T(2,128)(2,1)} %pad_maximum_fusion), calls=%async_computation.1 | async-start | bytes 262144 | tf_op jit(solution)/shard_map/all_to_all | solution.py:118
  63.6 18.8 %collective-permute-start = (bf16[64,16,128]{2,1,0:T(8,128)(2,1)}, bf16[64,16,128]{2,1,0:T(8,128)(2,1)}, u32[]{:S(2)}, u32[]{:S(2)}) collective-permute-start(bf16[64,16,128]{2,1,0:T(8,128)(2,1)} %slice.104), channel_id=1, source_target_pairs={{0,2},{2,4},{4,6},{6,0},{1,3},{3,5},{5,7},{7,1},{8,10},{10,12},{12... | collective-permute-start | bytes 786440 | tf_op jit(solution)/shard_map/ppermute | solution.py:125
  67.0 16.4 %collective-permute-start.1 = (bf16[64,16,128]{2,1,0:T(8,128)(2,1)}, bf16[64,16,128]{2,1,0:T(8,128)(2,1)}, u32[]{:S(2)}, u32[]{:S(2)}) collective-permute-start(bf16[64,16,128]{2,1,0:T(8,128)(2,1)} %slice.104), channel_id=1, source_target_pairs={{0,4},{2,6},{4,0},{6,2},{1,5},{3,7},{5,1},{7,3},{8,12},{10,14},{12... | collective-permute-start | bytes 786440 | tf_op jit(solution)/shard_map/ppermute | solution.py:125
  71.6 12.8 %collective-permute-start.2 = (bf16[64,16,128]{2,1,0:T(8,128)(2,1)}, bf16[64,16,128]{2,1,0:T(8,128)(2,1)S(1)}, u32[]{:S(2)}, u32[]{:S(2)}) collective-permute-start(bf16[64,16,128]{2,1,0:T(8,128)(2,1)} %slice.104), channel_id=1, source_target_pairs={{0,6},{2,0},{4,2},{6,4},{1,7},{3,1},{5,3},{7,5},{8,14},{10,8},{12,... | collective-permute-start | bytes 786440 | tf_op jit(solution)/shard_map/ppermute | solution.py:125
  75.0 48.0 %collective-permute-start.3 = (bf16[2048,128]{1,0:T(8,128)(2,1)}, bf16[2048,128]{1,0:T(8,128)(2,1)}, u32[]{:S(2)}, u32[]{:S(2)}) collective-permute-start(bf16[2048,128]{1,0:T(8,128)(2,1)} %bitcast.2), channel_id=1, source_target_pairs={{0,1},{1,0},{2,3},{3,2},{4,5},{5,4},{6,7},{7,6},{8,9},{9,8},{10,11... | collective-permute-start | bytes 1572872 | tf_op jit(solution)/shard_map/ppermute | solution.py:119
  78.3 9.5 %copy-start.3 = (f32[8,256]{1,0:T(8,128)S(1)}, f32[8,256]{1,0:T(8,128)}, u32[]{:S(2)}) copy-start(f32[8,256]{1,0:T(8,128)} %get-tuple-element.12) | copy-start | bytes 24580
  78.3 16.2 %copy-start.7 = (pred[128]{0:T(512)(128)(4,1)S(1)}, pred[128]{0:T(512)(128)(4,1)}, u32[]{:S(2)}) copy-start(pred[128]{0:T(512)(128)(4,1)} %get-tuple-element.23) | copy-start | bytes 388
  78.3 16.2 %copy-start.8 = (pred[128]{0:T(512)(128)(4,1)S(1)}, pred[128]{0:T(512)(128)(4,1)}, u32[]{:S(2)}) copy-start(pred[128]{0:T(512)(128)(4,1)} %get-tuple-element.24) | copy-start | bytes 388
  78.3 16.2 %copy-start.9 = (pred[2]{0:T(512)(128)(4,1)S(1)}, pred[2]{0:T(512)(128)(4,1)}, u32[]{:S(2)}) copy-start(pred[2]{0:T(512)(128)(4,1)} %iota_compare_fusion.7) | copy-start | bytes 10
  78.4 43.8 %copy-start.2 = (f32[32,256]{1,0:T(8,128)S(1)}, f32[32,256]{1,0:T(8,128)}, u32[]{:S(2)}) copy-start(f32[32,256]{1,0:T(8,128)} %param.17) | copy-start | bytes 98308
  78.4 43.8 %copy-start.4 = (bf16[32,128]{1,0:T(8,128)(2,1)S(1)}, bf16[32,128]{1,0:T(8,128)(2,1)}, u32[]{:S(2)}) copy-start(bf16[32,128]{1,0:T(8,128)(2,1)} %fusion.16) | copy-start | bytes 24580
  79.0 8.7 %all-to-all-start.2 = ((f32[8,2,512]{2,1,0:T(2,128)}), f32[8,2,512]{2,1,0:T(2,128)S(1)}, u32[]{:S(2)}, u32[]{:S(2)}) async-start(f32[8,2,512]{2,1,0:T(2,128)} %broadcast_in_dim.75), calls=%async_computation.2 | async-start | bytes 65536 | tf_op jit(solution)/shard_map/all_to_all | solution.py:20
  95.4 25.1 %all-to-all-start.3 = ((bf16[64,2,640]{2,1,0:T(2,128)(2,1)}), bf16[64,2,640]{2,1,0:T(2,128)(2,1)S(1)}, u32[]{:S(2)}, u32[]{:S(2)}) async-start(bf16[64,2,640]{2,1,0:T(2,128)(2,1)} %broadcast_in_dim.81), calls=%async_computation.3 | async-start | bytes 327680 | tf_op jit(solution)/shard_map/all_to_all | solution.py:20
  122.1 2.5 %copy-start.1 = (f32[64,4,2,8,128]{4,3,2,1,0:T(8,128)S(1)}, f32[64,4,2,8,128]{4,3,2,1,0:T(8,128)}, u32[]{:S(2)}) copy-start(f32[64,4,2,8,128]{4,3,2,1,0:T(8,128)} %bitcast_convert_fusion) | copy-start | bytes 6291460

commit v2 on v1

v2 whole, which is shorter than its diff:
```python
import jax
import jax.numpy as jnp
from jax import lax
from jax.experimental import pallas as pl
from jax.experimental.pallas import tpu as pltpu
from jax.sharding import PartitionSpec as P


RANK = 256
KW = 512
BF16 = jnp.bfloat16
F32 = jnp.float32


def dot32(left, right):
    return jnp.dot(left, right, preferred_element_type=F32)


def sent_to_all(value, axis, count):
    return lax.all_to_all(
        jnp.broadcast_to(value[None], (count, *value.shape)), axis, 0, 0, tiled=True
    )


def dot_rows(left, right):
    return lax.dot_general(left, right, (((1,), (1,)), ((), ())), preferred_element_type=F32)


def key_gradient_body(scale_ref, query_ref, key_ref, value_ref, grad_ref, out_ref):
    length = query_ref.shape[0]
    block = length // 2
    heads = scale_ref.shape[0]
    dim = query_ref.shape[1] // heads
    wide = value_ref.shape[1] // heads
    inv_root = dim ** (-0.5)
    pair = 2 * dim
    lane = lax.broadcasted_iota(jnp.int32, (block, pair), 1)
    later = lax.broadcasted_iota(jnp.int32, (block, block), 0) > lax.broadcasted_iota(
        jnp.int32, (block, block), 1
    )
    for first in range(0, heads, 2):
        lanes = slice(first * dim, first * dim + pair)
        found = [[], []]
        for side in range(2):
            head = first + side
            span = slice(head * wide, head * wide + wide)
            for step in range(2):
                rows = slice(step * block, step * block + block)
                seen = block * (step + 1)
                own = query_ref[rows, lanes].astype(F32) * inv_root
                own = jnp.where((lane >= dim) == (side == 1), own, 0.0).astype(BF16)
                scores = dot_rows(key_ref[:seen, lanes], own)
                last = jnp.where(later, -1e30, scores[seen - block :])
                scores = jnp.concatenate([scores[: seen - block], last], axis=0) if step else last
                exps = jnp.exp(scores - jnp.max(scores, axis=0, keepdims=True))
                total = jnp.sum(exps, axis=0, keepdims=True)
                attn_grad = dot_rows(value_ref[:seen, span], grad_ref[rows, span])
                weights_map = exps / total
                inner = jnp.sum(weights_map * attn_grad, axis=0, keepdims=True)
                score_grad = (-scale_ref[head] * weights_map * (attn_grad - inner)).astype(BF16)
                for place in range(step + 1):
                    found[place].append(
                        dot32(score_grad[place * block : place * block + block], own)
                    )
        for place in range(2):
            total = found[place][0]
            for more in found[place][1:]:
                total = total + more
            out_ref[place * block : place * block + block, lanes] = total.astype(BF16)


def key_gradient(query_rows, key_rows, value_rows, grad_rows, second_scale):
    return pl.pallas_call(
        key_gradient_body,
        out_shape=jax.ShapeDtypeStruct(query_rows.shape, BF16),
        in_specs=[pl.BlockSpec(memory_space=pltpu.SMEM)] + 4 * [pl.BlockSpec(memory_space=pltpu.VMEM)],
        out_specs=pl.BlockSpec(memory_space=pltpu.VMEM),
        name="key_gradient",
    )(second_scale, query_rows, key_rows, value_rows, grad_rows)


def first_message_body(place_ref, factor_ref, weight_ref, out_ref, own_ref):
    shards = out_ref.shape[0]
    rows, rank = factor_ref.shape
    half = rank // 2
    share = (out_ref.shape[1] - rows) // 2
    core = place_ref[0]
    ranks = lax.broadcasted_iota(jnp.int32, (rank, half), 0)
    places = lax.broadcasted_iota(jnp.int32, (rank, half), 1)
    factor = factor_ref[...]
    mine = dot32(factor, (ranks == 2 * places + core).astype(F32).astype(BF16)).astype(BF16)
    other = dot32(factor, (ranks == 2 * places + 1 - core).astype(F32).astype(BF16)).astype(BF16)
    own_ref[:, :half] = mine
    own_ref[:, half:] = other
    old = weight_ref[pl.ds(pl.multiple_of(place_ref[1] * share, share), share), :].astype(BF16)
    out_ref[:, :rows, :] = jnp.broadcast_to(mine[None], (shards, rows, half))
    for i in range(2):
        piece = old[:, i * half : i * half + half]
        out_ref[:, rows + i * share : rows + i * share + share, :] = jnp.broadcast_to(
            piece[None], (shards, share, half)
        )


def first_message(places, factor, weight, shards, reps):
    rows, rank = factor.shape
    half = rank // 2
    return pl.pallas_call(
        first_message_body,
        out_shape=(
            jax.ShapeDtypeStruct((shards, rows + 2 * (rows // reps), half), BF16),
            jax.ShapeDtypeStruct((rows, rank), BF16),
        ),
        in_specs=[pl.BlockSpec(memory_space=pltpu.SMEM)] + 2 * [pl.BlockSpec(memory_space=pltpu.VMEM)],
        out_specs=2 * (pl.BlockSpec(memory_space=pltpu.VMEM),),
        name="first_message",
    )(places, factor, weight)


def projected_sums_body(tokens_ref, factor_ref, grad_ref, out_ref):
    cols = grad_ref.shape[2]
    reduced = dot32(tokens_ref[...], factor_ref[...]).T
    high = reduced.astype(BF16)
    low = (reduced - high.astype(F32)).astype(BF16)
    for i in range(2):
        grads = grad_ref[i]
        out_ref[:, i * cols : i * cols + cols] = (dot32(high, grads) + dot32(low, grads)).astype(BF16)


def projected_sums(tokens, factor, grads):
    half = factor.shape[1]
    return pl.pallas_call(
        projected_sums_body,
        out_shape=jax.ShapeDtypeStruct((half, 2 * grads.shape[2]), BF16),
        in_specs=3 * [pl.BlockSpec(memory_space=pltpu.VMEM)],
        out_specs=pl.BlockSpec(memory_space=pltpu.VMEM),
        name="projected_sums",
    )(tokens, factor, grads)


def moments_step_body(place_ref, part_ref, moments_ref, message_ref, first_ref, second_ref):
    own_rows, cols = first_ref.shape
    pairs = own_rows // 2
    core = place_ref[0]
    part = part_ref[...]
    total = part[:own_rows]
    for i in range(own_rows, part.shape[0], own_rows):
        total = total + part[i : i + own_rows]
    order = [parity * pairs + place for place in range(pairs) for parity in range(2)]
    projected = jnp.concatenate([total[i : i + 1] for i in order], axis=0)
    both = [
        jnp.concatenate([moments_ref[0, rows, :], moments_ref[1, rows, :]], axis=1)
        for rows in (slice(0, own_rows), slice(own_rows, 2 * own_rows))
    ]
    new_first = 0.9 * both[0] + 0.1 * projected
    new_second = 0.95 * both[1] + 0.05 * projected * projected
    direction = (new_first / (jnp.sqrt(new_second) + 1e-08)).astype(BF16).astype(F32)
    squares = direction * direction
    squares = jnp.sum(jnp.sum(squares, axis=1, keepdims=True), axis=0, keepdims=True)

    def own_cols(value):
        return jnp.where(core == 0, value[:, :cols], value[:, cols:])

    first_ref[...] = own_cols(new_first)
    second_ref[...] = own_cols(new_second)
    own = own_cols(direction)
    for place in range(pairs):
        for parity in range(2):
            row = 2 * place + parity
            message_ref[place : place + 1, parity * cols : parity * cols + cols] = own[row : row + 1]
    high = squares.astype(BF16).astype(F32)
    middle = (squares - high).astype(BF16).astype(F32)
    low = squares - high - middle
    lane = lax.broadcasted_iota(jnp.int32, (pairs, 128), 1)
    row = lax.broadcasted_iota(jnp.int32, (pairs, 128), 0)
    packed = jnp.where(lane == 0, high, jnp.where(lane == 1, middle, jnp.where(lane == 2, low, 0.0)))
    message_ref[:, 2 * cols :] = jnp.where(row == 0, packed, 0.0)


def moments_step(places, part, moments):
    own_rows = moments.shape[1] // 2
    cols = moments.shape[2]
    return pl.pallas_call(
        moments_step_body,
        out_shape=(
            jax.ShapeDtypeStruct((own_rows // 2, 2 * cols + 128), F32),
            jax.ShapeDtypeStruct((own_rows, cols), F32),
            jax.ShapeDtypeStruct((own_rows, cols), F32),
        ),
        in_specs=[pl.BlockSpec(memory_space=pltpu.SMEM)] + 2 * [pl.BlockSpec(memory_space=pltpu.VMEM)],
        out_specs=3 * (pl.BlockSpec(memory_space=pltpu.VMEM),),
        name="moments_step",
    )(places, part, moments)


def on_device(
    tokens_in,
    query_two,
    key_two,
    values,
    out_grad,
    second_scale,
    factor,
    weight,
    first_moment,
    second_moment,
):
    shards = lax.axis_size("fs")
    reps = lax.axis_size("rep")
    core = lax.axis_index("tp")
    rank = factor.shape[1]
    half = rank // 2
    own_rows = first_moment.shape[0]
    pairs = own_rows // 2
    rows_here, cols = weight.shape

    places = jnp.stack([core, lax.axis_index("rep")])
    message, own_factor = first_message(places, factor, weight, shards, reps)
    share = rows_here // reps
    rep = lax.axis_index("rep")
    first_sent = lax.all_to_all(message, "fs", 0, 0, tiled=True)
    factor_mine = first_sent[:, :rows_here].reshape(-1, half)
    old_mine = first_sent[:, rows_here:]

    moments = lax.all_gather(jnp.concatenate([first_moment, second_moment], 0), "tp")
    moments = moments.reshape(2, 2 * own_rows, cols)

    key_grad = key_gradient(query_two, key_two, values, out_grad, second_scale)
    key_both = lax.all_gather(key_grad, "tp")

    sums = projected_sums(tokens_in, factor_mine, key_both)

    arrived = lax.all_to_all(sums.reshape(shards, pairs, 2 * cols), "fs", 0, 0, tiled=True)
    factor_other = lax.ppermute(factor_mine, "tp", [(0, 1), (1, 0)])
    factor_all = jnp.concatenate([factor_mine, factor_other], axis=1)
    old_all = jnp.zeros((shards, reps, *old_mine.shape[1:]), BF16)
    old_all = lax.dynamic_update_index_in_dim(old_all, old_mine, rep, 1)
    for i in range(1, reps):
        came = lax.ppermute(old_mine, "rep", [(j, (j + i) % reps) for j in range(reps)])
        old_all = lax.dynamic_update_index_in_dim(old_all, came, (rep + reps - i) % reps, 1)
    old_all = old_all.reshape(shards, reps, cols // half, share, half)
    old_weight = jnp.moveaxis(old_all, 2, 3).reshape(-1, cols)

    part = jnp.sum(arrived.astype(F32), axis=0)
    part = sent_to_all(part, ("rep", "tp"), 2 * reps)
    message, new_first, new_second = moments_step(
        places, part.reshape(reps * own_rows, 2 * cols), moments
    )
    gathered = sent_to_all(message.astype(BF16), "fs", shards)
    squares = jnp.sum(gathered[:, :, 2 * cols :].astype(F32))
    even = gathered[:, :, :cols].reshape(-1, cols)
    odd = gathered[:, :, cols : 2 * cols].reshape(-1, cols)
    rows = jnp.concatenate(
        [jnp.where(core == 0, even, odd), jnp.where(core == 0, odd, even)], axis=0
    )

    rate = lax.rsqrt(squares / (RANK * KW) + 1e-06)
    update_step = dot32(own_factor, rows) * rate
    new_weight = weight - 0.1 * update_step
    copies = (old_weight.astype(F32) - 0.1 * (dot32(factor_all, rows) * rate)).astype(BF16)
    return (new_weight, copies, update_step, new_first, new_second)


def solution(mesh):
    in_specs = (
        P(("fs", "rep"), None),
        P(("fs", "rep"), "tp"),
        P(("fs", "rep"), "tp"),
        P(("fs", "rep"), "tp"),
        P(("fs", "rep"), "tp"),
        P("tp"),
        P("fs", None),
        P("fs", "tp"),
        P("fs", "tp"),
        P("fs", "tp"),
    )
    out_specs = (P("fs", "tp"), P(None, "tp"), P("fs", "tp"), P("fs", "tp"), P("fs", "tp"))

    return jax.shard_map(on_device, mesh=mesh, in_specs=in_specs, out_specs=out_specs, check_vma=False)
```

time: 127 us -> 117 us (0.921)
  matrix products: 21.4 us -> 2.41 us
  waiting for transfers between devices: 13.7 us -> 32.5 us
  Pallas kernels: 0 us -> 12.1 us
  local copies, waits for them, and re-layouts: 13.2 us -> 5.02 us
  starting transfers between devices: 58 us -> 52.4 us
  between operations: 7.22 us -> 1.63 us
  other arithmetic: 8.27 us -> 3.84 us
  blocking collectives: 3.99 us -> 5.76 us
    all_to_all x3 -> x2, starting transfers between devices: 32.8 us -> 16 us  [sent_to_all(): lax.all_to_all(jnp.broadcast_to(value[None], (count, *value.shape)), axis...]
    all_to_all x0 -> x1, starting transfers between devices: none -> 16.6 us  [on_device(): first_sent = lax.all_to_all(message, 'fs', 0, 0, tiled=True)]
    all_to_all x0 -> x1, waiting for transfers between devices: none -> 15.2 us  [on_device(): first_sent = lax.all_to_all(message, 'fs', 0, 0, tiled=True)]
    pallas_call x0 -> x4, Pallas kernels: none -> 12.1 us  [the longest x1 4.99 us: key_gradient(): pl.pallas_call(key_gradient_body, out_shape=jax.ShapeDtypeStruct(query_ro...]
    dot_general x6 -> x0, matrix products: 8.92 us -> none  [the longest x1 4.3 us: key_gradient(): jnp.einsum('hqk,qhd->khd', score_grad, queries, preferred_element_type=jn...]
    div x1 -> x0, matrix products: 6.64 us -> none  [key_gradient(): weights_map = exps / jnp.sum(exps, axis=-1, keepdims=True)]
    all_to_all x1, starting transfers between devices: 11.9 us -> 6.52 us  [on_device(): lax.all_to_all(sums.reshape(shards, pairs, 2 * cols), 'fs', 0, 0, tiled=T...]
    dot_general x5 -> x2, matrix products: 5.88 us -> 2.41 us  [dot32(): return jnp.dot(left, right, preferred_element_type=F32)]
  transfers between devices with their start and end apart: 8 -> 8, of which waited for: 3 -> 4; matrix products, arithmetic and copies ran while one was open for 25% -> 4% of each run, Pallas kernels for 0% -> 6%
where the time goes in v2:
time: 117 us; the launch traced here: 116 us
  starting transfers between devices  52.4 us (45%)
  waiting for transfers between devices  32.5 us (28%)
  Pallas kernels  12.1 us (10%)
  blocking collectives  5.76 us (5%)
  local copies, waits for them, and re-layouts  5.02 us (4%)
  other arithmetic  3.84 us (3%)
  matrix products  2.41 us (2%)
  between operations  1.63 us (1%)
    all_to_all x2, waiting for transfers between devices, sent_to_all(): lax.all_to_all(jnp.broadcast_to(value[None], (count, *value.shape)), axis...  17.1 us
    all_to_all x1, starting transfers between devices, on_device(): first_sent = lax.all_to_all(message, 'fs', 0, 0, tiled=True)  16.6 us
    all_to_all x2, starting transfers between devices, sent_to_all(): lax.all_to_all(jnp.broadcast_to(value[None], (count, *value.shape)), axis...  16 us
    all_to_all x1, waiting for transfers between devices, on_device(): first_sent = lax.all_to_all(message, 'fs', 0, 0, tiled=True)  15.2 us
    ppermute x3, starting transfers between devices, on_device(): lax.ppermute(old_mine, 'rep', [(j, (j + i) % reps) for j in range(reps)])  11.4 us
    all_to_all x1, starting transfers between devices, on_device(): lax.all_to_all(sums.reshape(shards, pairs, 2 * cols), 'fs', 0, 0, tiled=T...  6.52 us
    pallas_call x1, Pallas kernels, key_gradient(): pl.pallas_call(key_gradient_body, out_shape=jax.ShapeDtypeStruct(query_ro...  4.99 us
    all_gather x1, blocking collectives, on_device(): key_both = lax.all_gather(key_grad, 'tp')  3.81 us
  transfers between devices with their start and end apart: 8, of which 4 were waited for; matrix products, arithmetic and copies ran while one was open for 4% of the time, Pallas kernels for 6%

profile of v2, /device:TPU:8, one launch (start us, length us, event | category | flops | bytes accessed | tf_op | source)
XLA Modules:
  0.0 115.7 jit_solution(2796711422592208650)
XLA Ops:
  0.6 0.7 pad_add_fusion.place_ref
  1.3 1.8 %first_message.1 = (bf16[64,48,128]{2,1,0:T(8,128)(2,1)}, bf16[32,256]{1,0:T(8,128)(2,1)}) custom-call(s32[2]{0:T(128)} %pad_add_fusion.place_ref, bf16[32,256]{1,0:T(8,128)(2,1)} %factor_ref.1, f32[32,256]{1,0:T(8,128)} %weight_ref.1), custom_call_target="tpu_custom_call" | custom-call | tf_op jit(solution)/shard_map/first_message/pallas_call | solution.py:107
  3.1 16.6 %all-to-all-start = ((bf16[64,48,128]{2,1,0:T(8,128)(2,1)}), bf16[64,48,128]{2,1,0:T(8,128)(2,1)S(1)}, u32[]{:S(2)}, u32[]{:S(2)}) async-start(bf16[64,48,128]{2,1,0:T(8,128)(2,1)} %get-tuple-element.11), calls=%async_computation | async-start | bytes 1572864 | tf_op jit(solution)/shard_map/all_to_all | solution.py:220
  19.7 5.0 %key_gradient.1 = bf16[512,256]{1,0:T(8,128)(2,1)} custom-call(f32[4]{0:T(128)} %scale_ref.1, bf16[512,256]{1,0:T(8,128)(2,1)} %query_ref.1, bf16[512,256]{1,0:T(8,128)(2,1)} %key_ref.1, bf16[512,512]{1,0:T(8,128)(2,1)} %value_ref.1, bf16[512,512]{1,0:T(8,128)(2,1)} %grad_ref.1), custom_call_target="tpu_custom_call" | custom-call | tf_op jit(solution)/shard_map/key_gradient/pallas_call | solution.py:73
  24.7 3.8 %all-gather = bf16[1024,256]{1,0:T(8,128)(2,1)} all-gather(bf16[512,256]{1,0:T(8,128)(2,1)} %key_gradient.1), channel_id=2, replica_groups=mesh['fs'=64,'rep'=4,'tp'=2] {'tp'}, dimensions={0}, use_global_device_ids=true | all-gather | bytes 786432 | tf_op jit(solution)/shard_map/all_gather | solution.py:228
  28.5 15.2 %all-to-all-done = bf16[64,48,128]{2,1,0:T(8,128)(2,1)S(1)} async-done(((bf16[64,48,128]{2,1,0:T(8,128)(2,1)}), bf16[64,48,128]{2,1,0:T(8,128)(2,1)S(1)}, u32[]{:S(2)}, u32[]{:S(2)}) %all-to-all-start) | async-done | bytes 786464 | tf_op jit(solution)/shard_map/all_to_all | solution.py:220
  43.7 0.8 slice.20
  44.5 0.0 copy-start.2
  44.5 0.0 copy-start.3
  44.5 3.8 %projected_sums.1 = bf16[128,512]{1,0:T(8,128)(2,1)} custom-call(bf16[512,2048]{1,0:T(8,128)(2,1)} %tokens_ref.1, bf16[2048,128]{1,0:T(8,128)(2,1)} %bitcast.2.factor_ref, bf16[2,512,256]{2,1,0:T(8,128)(2,1)} %bitcast.31), custom_call_target="tpu_custom_call" | custom-call | tf_op jit(solution)/shard_map/projected_sums/pallas_call | solution.py:131
  48.3 1.6 %reshape.34 = bf16[64,2,512]{2,1,0:T(2,128)(2,1)} reshape(bf16[128,512]{1,0:T(8,128)(2,1)} %projected_sums.1) | data formatting | bytes 262144 | tf_op jit(solution)/shard_map/reshape | solution.py:232
  49.9 6.5 %all-to-all-start.1 = ((bf16[64,2,512]{2,1,0:T(2,128)(2,1)}), bf16[64,2,512]{2,1,0:T(2,128)(2,1)S(1)}, u32[]{:S(2)}, u32[]{:S(2)}) async-start(bf16[64,2,512]{2,1,0:T(2,128)(2,1)} %reshape.34), calls=%async_computation.1 | async-start | bytes 262144 | tf_op jit(solution)/shard_map/all_to_all | solution.py:232
  56.4 0.0 copy-done.2
  56.4 0.0 copy-done.3
  56.5 2.0 %all-gather.1 = f32[16,256]{1,0:T(8,128)} all-gather(f32[8,256]{1,0:T(8,128)S(1)} %pad_maximum_fusion), channel_id=3, replica_groups=mesh['fs'=64,'rep'=4,'tp'=2] {'tp'}, dimensions={0}, use_global_device_ids=true | all-gather | bytes 24576 | tf_op jit(solution)/shard_map/all_gather | solution.py:224
  58.5 3.4 %collective-permute-start = (bf16[64,16,128]{2,1,0:T(8,128)(2,1)S(1)}, bf16[64,16,128]{2,1,0:T(8,128)(2,1)S(1)}, u32[]{:S(2)}, u32[]{:S(2)}) collective-permute-start(bf16[64,16,128]{2,1,0:T(8,128)(2,1)S(1)} %slice.24), channel_id=1, source_target_pairs={{0,2},{2,4},{4,6},{6,0},{1,3},{3,5},{5,7},{7,1},{8,10},{10,12},{12... | collective-permute-start | bytes 786440 | tf_op jit(solution)/shard_map/ppermute | solution.py:238
  61.9 4.6 %collective-permute-start.1 = (bf16[64,16,128]{2,1,0:T(8,128)(2,1)S(1)}, bf16[64,16,128]{2,1,0:T(8,128)(2,1)S(1)}, u32[]{:S(2)}, u32[]{:S(2)}) collective-permute-start(bf16[64,16,128]{2,1,0:T(8,128)(2,1)S(1)} %slice.24), channel_id=1, source_target_pairs={{0,4},{2,6},{4,0},{6,2},{1,5},{3,7},{5,1},{7,3},{8,12},{10,14},{12... | collective-permute-start | bytes 786440 | tf_op jit(solution)/shard_map/ppermute | solution.py:238
  66.5 3.3 %collective-permute-start.2 = (bf16[64,16,128]{2,1,0:T(8,128)(2,1)S(1)}, bf16[64,16,128]{2,1,0:T(8,128)(2,1)S(1)}, u32[]{:S(2)}, u32[]{:S(2)}) collective-permute-start(bf16[64,16,128]{2,1,0:T(8,128)(2,1)S(1)} %slice.24), channel_id=1, source_target_pairs={{0,6},{2,0},{4,2},{6,4},{1,7},{3,1},{5,3},{7,5},{8,14},{10,8},{12,... | collective-permute-start | bytes 786440 | tf_op jit(solution)/shard_map/ppermute | solution.py:238
  69.9 1.9 %collective-permute-start.3 = (bf16[2048,128]{1,0:T(8,128)(2,1)}, bf16[2048,128]{1,0:T(8,128)(2,1)}, u32[]{:S(2)}, u32[]{:S(2)}) collective-permute-start(bf16[2048,128]{1,0:T(8,128)(2,1)} %bitcast.2.factor_ref), channel_id=1, source_target_pairs={{0,1},{1,0},{2,3},{3,2},{4,5},{5,4},{6,7},{7,6},{8,9},{9,8},{10,11... | collective-permute-start | bytes 1572872 | tf_op jit(solution)/shard_map/ppermute | solution.py:233
  71.8 0.2 broadcast_in_dim.30
  72.1 0.0 all-to-all-done.1
  72.1 0.1 convert_reduce_fusion
  72.3 0.6 broadcast_in_dim.28
  72.9 3.3 %all-to-all-start.2 = ((f32[8,2,512]{2,1,0:T(2,128)}), f32[8,2,512]{2,1,0:T(2,128)S(1)}, u32[]{:S(2)}, u32[]{:S(2)}) async-start(f32[8,2,512]{2,1,0:T(2,128)} %broadcast_in_dim.28), calls=%async_computation.2 | async-start | bytes 65536 | tf_op jit(solution)/shard_map/all_to_all | solution.py:20
  76.3 0.0 collective-permute-done
  76.3 0.2 collective-permute-done.1
  76.6 5.0 %all-to-all-done.2 = f32[8,2,512]{2,1,0:T(2,128)S(1)} async-done(((f32[8,2,512]{2,1,0:T(2,128)}), f32[8,2,512]{2,1,0:T(2,128)S(1)}, u32[]{:S(2)}, u32[]{:S(2)}) %all-to-all-start.2) | async-done | bytes 32800 | tf_op jit(solution)/shard_map/all_to_all | solution.py:20
  81.6 0.6 reshape.35.part_ref
  82.3 1.5 %moments_step.1 = (f32[2,640]{1,0:T(2,128)}, f32[4,256]{1,0:T(4,128)}, f32[4,256]{1,0:T(4,128)}) custom-call(s32[2]{0:T(128)} %pad_add_fusion.place_ref, f32[16,512]{1,0:T(8,128)} %reshape.35.part_ref, f32[2,8,256]{2,1,0:T(8,128)} %bitcast.32), custom_call_target="tpu_custom_call" | custom-call | tf_op jit(solution)/shard_map/moments_step/pallas_call | solution.py:182
  83.8 0.7 convert_element_type.25
  84.4 0.8 broadcast_in_dim.29
  85.2 12.7 %all-to-all-start.3 = ((bf16[64,2,640]{2,1,0:T(2,128)(2,1)}), bf16[64,2,640]{2,1,0:T(2,128)(2,1)S(1)}, u32[]{:S(2)}, u32[]{:S(2)}) async-start(bf16[64,2,640]{2,1,0:T(2,128)(2,1)} %broadcast_in_dim.29), calls=%async_computation.3 | async-start | bytes 327680 | tf_op jit(solution)/shard_map/all_to_all | solution.py:20
  97.9 0.0 collective-permute-done.2
  98.0 0.0 copy-start
  98.0 0.0 copy-start.1
  98.0 0.2 bitcast_convert_fusion
  98.3 12.1 %all-to-all-done.3 = bf16[64,2,640]{2,1,0:T(2,128)(2,1)S(1)} async-done(((bf16[64,2,640]{2,1,0:T(2,128)(2,1)}), bf16[64,2,640]{2,1,0:T(2,128)(2,1)S(1)}, u32[]{:S(2)}, u32[]{:S(2)}) %all-to-all-start.3) | async-done | bytes 163872 | tf_op jit(solution)/shard_map/all_to_all | solution.py:20
  110.3 0.1 broadcast_select_fusion
  110.6 0.6 convert_reduce_fusion.1
  111.9 0.0 copy-done
  111.9 0.0 copy-done.1
  111.9 0.8 multiply_subtract_fusion
  112.7 0.0 collective-permute-done.3
  112.7 1.6 %fusion = f32[2048,256]{1,0:T(8,128)S(1)} fusion(bf16[256,256]{1,0:T(8,128)(2,1)S(1)} %constant_dynamic-update-slice_fusion, bf16[2048,128]{1,0:T(8,128)(2,1)} %collective-permute-done.3, bf16[2048,128]{1,0:T(8,128)(2,1)} %bitcast.2.factor_ref, f32[]{:T(128)S(6)} %rsqrt.3), kind=kOutput, calls=%fused_computation.1 | convolution fusion | flops 271581184 | bytes 3276804 | tf_op jit(solution)/shard_map/dot_general | solution.py:16
  114.3 1.4 %subtract_convert_fusion = bf16[2048,256]{1,0:T(8,128)(2,1)} fusion(f32[2048,256]{1,0:T(8,128)S(1)} %bitcast.30, f32[2048,256]{1,0:T(8,128)S(1)} %fusion), kind=kLoop, calls=%fused_computation.2 | loop fusion | flops 1048576 | bytes 5242880 | tf_op jit(solution)/shard_map/convert_element_type | solution.py:259
  (11 shorter events, 0.3 us)
Async XLA Ops:
  3.1 40.6 %all-to-all-start = ((bf16[64,48,128]{2,1,0:T(8,128)(2,1)}), bf16[64,48,128]{2,1,0:T(8,128)(2,1)S(1)}, u32[]{:S(2)}, u32[]{:S(2)}) async-start(bf16[64,48,128]{2,1,0:T(8,128)(2,1)} %get-tuple-element.11), calls=%async_computation | async-start | bytes 1572864 | tf_op jit(solution)/shard_map/all_to_all | solution.py:220
  44.5 11.9 %copy-start.2 = (f32[4,256]{1,0:T(4,128)S(1)}, f32[4,256]{1,0:T(4,128)}, u32[]{:S(2)}) copy-start(f32[4,256]{1,0:T(4,128)} %param.19) | copy-start | bytes 12292
  44.5 11.9 %copy-start.3 = (f32[4,256]{1,0:T(4,128)S(1)}, f32[4,256]{1,0:T(4,128)}, u32[]{:S(2)}) copy-start(f32[4,256]{1,0:T(4,128)} %param.18) | copy-start | bytes 12292
  49.9 22.2 %all-to-all-start.1 = ((bf16[64,2,512]{2,1,0:T(2,128)(2,1)}), bf16[64,2,512]{2,1,0:T(2,128)(2,1)S(1)}, u32[]{:S(2)}, u32[]{:S(2)}) async-start(bf16[64,2,512]{2,1,0:T(2,128)(2,1)} %reshape.34), calls=%async_computation.1 | async-start | bytes 262144 | tf_op jit(solution)/shard_map/all_to_all | solution.py:232
  58.5 17.8 %collective-permute-start = (bf16[64,16,128]{2,1,0:T(8,128)(2,1)S(1)}, bf16[64,16,128]{2,1,0:T(8,128)(2,1)S(1)}, u32[]{:S(2)}, u32[]{:S(2)}) collective-permute-start(bf16[64,16,128]{2,1,0:T(8,128)(2,1)S(1)} %slice.24), channel_id=1, source_target_pairs={{0,2},{2,4},{4,6},{6,0},{1,3},{3,5},{5,7},{7,1},{8,10},{10,12},{12... | collective-permute-start | bytes 786440 | tf_op jit(solution)/shard_map/ppermute | solution.py:238
  61.9 14.7 %collective-permute-start.1 = (bf16[64,16,128]{2,1,0:T(8,128)(2,1)S(1)}, bf16[64,16,128]{2,1,0:T(8,128)(2,1)S(1)}, u32[]{:S(2)}, u32[]{:S(2)}) collective-permute-start(bf16[64,16,128]{2,1,0:T(8,128)(2,1)S(1)} %slice.24), channel_id=1, source_target_pairs={{0,4},{2,6},{4,0},{6,2},{1,5},{3,7},{5,1},{7,3},{8,12},{10,14},{12... | collective-permute-start | bytes 786440 | tf_op jit(solution)/shard_map/ppermute | solution.py:238
  66.5 31.4 %collective-permute-start.2 = (bf16[64,16,128]{2,1,0:T(8,128)(2,1)S(1)}, bf16[64,16,128]{2,1,0:T(8,128)(2,1)S(1)}, u32[]{:S(2)}, u32[]{:S(2)}) collective-permute-start(bf16[64,16,128]{2,1,0:T(8,128)(2,1)S(1)} %slice.24), channel_id=1, source_target_pairs={{0,6},{2,0},{4,2},{6,4},{1,7},{3,1},{5,3},{7,5},{8,14},{10,8},{12,... | collective-permute-start | bytes 786440 | tf_op jit(solution)/shard_map/ppermute | solution.py:238
  69.9 42.8 %collective-permute-start.3 = (bf16[2048,128]{1,0:T(8,128)(2,1)}, bf16[2048,128]{1,0:T(8,128)(2,1)}, u32[]{:S(2)}, u32[]{:S(2)}) collective-permute-start(bf16[2048,128]{1,0:T(8,128)(2,1)} %bitcast.2.factor_ref), channel_id=1, source_target_pairs={{0,1},{1,0},{2,3},{3,2},{4,5},{5,4},{6,7},{7,6},{8,9},{9,8},{10,11... | collective-permute-start | bytes 1572872 | tf_op jit(solution)/shard_map/ppermute | solution.py:233
  72.9 8.7 %all-to-all-start.2 = ((f32[8,2,512]{2,1,0:T(2,128)}), f32[8,2,512]{2,1,0:T(2,128)S(1)}, u32[]{:S(2)}, u32[]{:S(2)}) async-start(f32[8,2,512]{2,1,0:T(2,128)} %broadcast_in_dim.28), calls=%async_computation.2 | async-start | bytes 65536 | tf_op jit(solution)/shard_map/all_to_all | solution.py:20
  85.2 25.1 %all-to-all-start.3 = ((bf16[64,2,640]{2,1,0:T(2,128)(2,1)}), bf16[64,2,640]{2,1,0:T(2,128)(2,1)S(1)}, u32[]{:S(2)}, u32[]{:S(2)}) async-start(bf16[64,2,640]{2,1,0:T(2,128)(2,1)} %broadcast_in_dim.29), calls=%async_computation.3 | async-start | bytes 327680 | tf_op jit(solution)/shard_map/all_to_all | solution.py:20
  98.0 13.9 %copy-start = (f32[32,256]{1,0:T(8,128)S(1)}, f32[32,256]{1,0:T(8,128)}, u32[]{:S(2)}) copy-start(f32[32,256]{1,0:T(8,128)} %weight_ref.1) | copy-start | bytes 98308
  98.0 13.9 %copy-start.1 = (bf16[32,256]{1,0:T(8,128)(2,1)S(1)}, bf16[32,256]{1,0:T(8,128)(2,1)}, u32[]{:S(2)}) copy-start(bf16[32,256]{1,0:T(8,128)(2,1)} %get-tuple-element.10) | copy-start | bytes 49156

commit v3 on v2

v3 whole, which is shorter than its diff:
```python
import jax
import jax.numpy as jnp
from jax import lax
from jax.experimental import pallas as pl
from jax.experimental.pallas import tpu as pltpu
from jax.sharding import PartitionSpec as P


RANK = 256
KW = 512
BF16 = jnp.bfloat16
F32 = jnp.float32

MIB = 1024 * 1024
VMEM_SPEC = pl.BlockSpec(memory_space=pltpu.VMEM)


def dot32(left, right):
    return jnp.dot(left, right, preferred_element_type=F32)


def dot_rows(left, right):
    return lax.dot_general(left, right, (((1,), (1,)), ((), ())), preferred_element_type=F32)


def key_gradient_body(scale_ref, query_ref, key_ref, value_ref, grad_ref, out_ref):
    length = query_ref.shape[0]
    block = length // 2
    heads = scale_ref.shape[0]
    dim = query_ref.shape[1] // heads
    wide = value_ref.shape[1] // heads
    inv_root = dim ** (-0.5)
    pair = 2 * dim
    lane = lax.broadcasted_iota(jnp.int32, (block, pair), 1)
    later = lax.broadcasted_iota(jnp.int32, (block, block), 0) > lax.broadcasted_iota(
        jnp.int32, (block, block), 1
    )
    for first in range(0, heads, 2):
        lanes = slice(first * dim, first * dim + pair)
        found = [[], []]
        for side in range(2):
            head = first + side
            span = slice(head * wide, head * wide + wide)
            for step in range(2):
                rows = slice(step * block, step * block + block)
                seen = block * (step + 1)
                own = query_ref[rows, lanes].astype(F32) * inv_root
                own = jnp.where((lane >= dim) == (side == 1), own, 0.0).astype(BF16)
                scores = dot_rows(key_ref[:seen, lanes], own)
                last = jnp.where(later, -1e30, scores[seen - block :])
                scores = jnp.concatenate([scores[: seen - block], last], axis=0) if step else last
                exps = jnp.exp(scores - jnp.max(scores, axis=0, keepdims=True))
                total = jnp.sum(exps, axis=0, keepdims=True)
                attn_grad = dot_rows(value_ref[:seen, span], grad_ref[rows, span])
                weights_map = exps / total
                inner = jnp.sum(weights_map * attn_grad, axis=0, keepdims=True)
                score_grad = (-scale_ref[head] * weights_map * (attn_grad - inner)).astype(BF16)
                for place in range(step + 1):
                    found[place].append(
                        dot32(score_grad[place * block : place * block + block], own)
                    )
        for place in range(2):
            total = found[place][0]
            for more in found[place][1:]:
                total = total + more
            out_ref[place * block : place * block + block, lanes] = total.astype(BF16)


def key_gradient(query_rows, key_rows, value_rows, grad_rows, second_scale):
    return pl.pallas_call(
        key_gradient_body,
        out_shape=jax.ShapeDtypeStruct(query_rows.shape, BF16),
        in_specs=[pl.BlockSpec(memory_space=pltpu.SMEM)] + 4 * [pl.BlockSpec(memory_space=pltpu.VMEM)],
        out_specs=pl.BlockSpec(memory_space=pltpu.VMEM),
        compiler_params=pltpu.CompilerParams(vmem_limit_bytes=24 * MIB),
        name="key_gradient",
    )(second_scale, query_rows, key_rows, value_rows, grad_rows)


def first_message_body(factor_ref, weight_ref, out_ref, own_ref):
    shards = out_ref.shape[0]
    rows, rank = factor_ref.shape
    half = rank // 2
    share = (out_ref.shape[1] - rows) // 2
    core = lax.axis_index("tp")
    ranks = lax.broadcasted_iota(jnp.int32, (rank, half), 0)
    places = lax.broadcasted_iota(jnp.int32, (rank, half), 1)
    pair = sum((places >= i * shards).astype(jnp.int32) for i in range(1, half // shards))
    wanted = (places - pair * shards) * (rank // shards) + 2 * pair
    factor = factor_ref[...]
    mine = dot32(factor, (ranks == wanted + core).astype(F32).astype(BF16)).astype(BF16)
    other = dot32(factor, (ranks == wanted + 1 - core).astype(F32).astype(BF16)).astype(BF16)
    own_ref[:, :half] = mine
    own_ref[:, half:] = other
    start = pl.multiple_of(lax.axis_index("rep") * share, share)
    old = weight_ref[pl.ds(start, share), :].astype(BF16)
    out_ref[:, :rows, :] = jnp.broadcast_to(mine[None], (shards, rows, half))
    for i in range(2):
        piece = old[:, i * half : i * half + half]
        out_ref[:, rows + i * share : rows + i * share + share, :] = jnp.broadcast_to(
            piece[None], (shards, share, half)
        )


def first_message(factor, weight, shards, reps):
    rows, rank = factor.shape
    half = rank // 2
    return pl.pallas_call(
        first_message_body,
        out_shape=(
            jax.ShapeDtypeStruct((shards, rows + 2 * (rows // reps), half), BF16),
            jax.ShapeDtypeStruct((rows, rank), BF16),
        ),
        in_specs=2 * [VMEM_SPEC],
        out_specs=(VMEM_SPEC, VMEM_SPEC),
        compiler_params=pltpu.CompilerParams(vmem_limit_bytes=8 * MIB),
        name="first_message",
    )(factor, weight)


def projected_sums_body(tokens_ref, sent_ref, grad_ref, out_ref, laid_ref):
    shards, _, half = sent_ref.shape
    length, width = tokens_ref.shape
    rows = width // shards
    cols = grad_ref.shape[1]
    pairs = half // shards
    factor = sent_ref[:, :rows, :].reshape(width, half)
    reduced = dot32(tokens_ref[...], factor).T
    high = reduced.astype(BF16)
    low = (reduced - high.astype(F32)).astype(BF16)
    tiles = cols // 128
    for i in range(2):
        grads = grad_ref[i * length : i * length + length, :]
        sums = dot32(high, grads) + dot32(low, grads)
        for pair in range(pairs):
            for tile in range(tiles):
                place = (pair * 2 + i) * tiles + tile
                laid_ref[pl.ds(place, shards, 2 * pairs * tiles), :] = sums[
                    pair * shards : pair * shards + shards, tile * 128 : tile * 128 + 128
                ]
    out_ref[...] = laid_ref[...].astype(BF16)


def projected_sums(tokens, sent, grads):
    half = sent.shape[2]
    total = half * 2 * grads.shape[1] // 128
    return pl.pallas_call(
        projected_sums_body,
        out_shape=jax.ShapeDtypeStruct((total, 128), BF16),
        in_specs=3 * [VMEM_SPEC],
        out_specs=VMEM_SPEC,
        scratch_shapes=[pltpu.VMEM((total, 128), F32)],
        cost_estimate=pl.CostEstimate(
            flops=4 * tokens.size * half, bytes_accessed=2 * tokens.size, transcendentals=0
        ),
        compiler_params=pltpu.CompilerParams(vmem_limit_bytes=16 * MIB),
        name="projected_sums",
    )(tokens, sent, grads)


def summed_body(arrived_ref, out_ref):
    total = jnp.sum(arrived_ref[...].astype(F32), axis=0)
    out_ref[...] = jnp.broadcast_to(total[None], out_ref.shape)


def summed(arrived, count):
    return pl.pallas_call(
        summed_body,
        out_shape=jax.ShapeDtypeStruct((count, *arrived.shape[1:]), F32),
        in_specs=[VMEM_SPEC],
        out_specs=VMEM_SPEC,
        compiler_params=pltpu.CompilerParams(vmem_limit_bytes=4 * MIB),
        name="summed",
    )(arrived)


def moments_step_body(part_ref, moments_ref, message_ref, first_ref, second_ref):
    shards = message_ref.shape[0]
    lines = first_ref.shape[0]
    core = lax.axis_index("tp")
    total = part_ref[:lines, :]
    for i in range(lines, part_ref.shape[0], lines):
        total = total + part_ref[i : i + lines, :]
    new_first = 0.9 * moments_ref[:lines, :] + 0.1 * total
    new_second = 0.95 * moments_ref[lines:, :] + 0.05 * total * total
    first_ref[...] = new_first
    second_ref[...] = new_second
    direction = (new_first / (jnp.sqrt(new_second) + 1e-08)).astype(BF16).astype(F32)
    squares = direction * direction
    squares = jnp.sum(jnp.sum(squares, axis=1, keepdims=True), axis=0, keepdims=True)
    quarter = lines // 8
    own = []
    for i in range(4):
        base = i * 2 * quarter
        own.append(
            jnp.where(
                core == 0,
                direction[base : base + quarter],
                direction[base + quarter : base + 2 * quarter],
            )
        )
    high = squares.astype(BF16).astype(F32)
    middle = (squares - high).astype(BF16).astype(F32)
    low = squares - high - middle
    lane = lax.broadcasted_iota(jnp.int32, (lines // 2, 128), 1)
    row = lax.broadcasted_iota(jnp.int32, (lines // 2, 128), 0)
    packed = jnp.where(lane == 0, high, jnp.where(lane == 1, middle, jnp.where(lane == 2, low, 0.0)))
    own.append(jnp.where(row == 0, packed, 0.0))
    message = jnp.concatenate(own, axis=0).astype(BF16)
    message_ref[...] = jnp.broadcast_to(message[None], (shards, lines, 128))


def moments_step(part, moments, shards):
    lines = moments.shape[0] // 2
    return pl.pallas_call(
        moments_step_body,
        out_shape=(
            jax.ShapeDtypeStruct((shards, lines, 128), BF16),
            jax.ShapeDtypeStruct((lines, 128), F32),
            jax.ShapeDtypeStruct((lines, 128), F32),
        ),
        in_specs=2 * [VMEM_SPEC],
        out_specs=3 * (VMEM_SPEC,),
        compiler_params=pltpu.CompilerParams(vmem_limit_bytes=4 * MIB),
        name="moments_step",
    )(part, moments)


def new_weights_body(
    gathered_ref, sent_ref, swapped_ref, old_ref, own_ref, weight_ref,
    copies_ref, update_ref, weight_out_ref, laid_ref,
):
    shards = sent_ref.shape[0]
    lines = gathered_ref.shape[0] // shards
    width, half = swapped_ref.shape
    rows = width // shards
    reps, share = copies_ref.shape[1:3]
    cols = weight_ref.shape[1]
    tiles = cols // 128
    pairs = half // shards
    core = lax.axis_index("tp")
    laid_ref[...] = gathered_ref[...].astype(F32)

    def line(place):
        return laid_ref[pl.ds(place, shards, lines), :]

    def directions(parity):
        return jnp.concatenate(
            [
                jnp.concatenate(
                    [line((parity * pairs + pair) * tiles + tile) for tile in range(tiles)], axis=1
                )
                for pair in range(pairs)
            ],
            axis=0,
        )

    even, odd = directions(0), directions(1)
    mine = jnp.where(core == 0, even, odd).astype(BF16)
    other = jnp.where(core == 0, odd, even).astype(BF16)
    squares = line(lines // 2)
    squares = jnp.sum(jnp.sum(squares, axis=1, keepdims=True), axis=0, keepdims=True)
    rate = lax.rsqrt(squares / (RANK * KW) + 1e-06)
    update = (dot32(own_ref[:, :half], mine) + dot32(own_ref[:, half:], other)) * rate
    update_ref[...] = update
    weight_out_ref[...] = weight_ref[...] - 0.1 * update
    pieces = 4
    group = shards // pieces
    for piece in range(pieces):
        owners = slice(piece * group, piece * group + group)
        factor = sent_ref[owners, :rows, :].reshape(group * rows, half)
        swapped = swapped_ref[piece * group * rows : (piece + 1) * group * rows, :]
        step = (dot32(factor, mine) + dot32(swapped, other)) * (0.1 * rate)
        for i in range(cols // half):
            lanes = slice(i * half, i * half + half)
            old = old_ref[owners, :, i * share : i * share + share, :].astype(F32)
            copies_ref[owners, :, :, lanes] = (
                old - step[:, lanes].reshape(group, reps, share, half)
            ).astype(BF16)


def new_weights(gathered, sent, swapped, old, own_factor, weight):
    shards, reps = old.shape[:2]
    rows, cols = weight.shape
    return pl.pallas_call(
        new_weights_body,
        out_shape=(
            jax.ShapeDtypeStruct((shards, reps, rows // reps, cols), BF16),
            jax.ShapeDtypeStruct((rows, cols), F32),
            jax.ShapeDtypeStruct((rows, cols), F32),
        ),
        in_specs=6 * [VMEM_SPEC],
        out_specs=3 * (VMEM_SPEC,),
        scratch_shapes=[pltpu.VMEM(gathered.shape, F32)],
        cost_estimate=pl.CostEstimate(
            flops=4 * swapped.size * cols, bytes_accessed=8 * swapped.size, transcendentals=0
        ),
        compiler_params=pltpu.CompilerParams(vmem_limit_bytes=20 * MIB),
        name="new_weights",
    )(gathered, sent, swapped, old, own_factor, weight)


def on_device(
    tokens_in,
    query_two,
    key_two,
    values,
    out_grad,
    second_scale,
    factor,
    weight,
    first_moment,
    second_moment,
):
    shards = lax.axis_size("fs")
    reps = lax.axis_size("rep")
    rep = lax.axis_index("rep")
    core = lax.axis_index("tp")
    half = factor.shape[1] // 2
    rows, cols = weight.shape
    tiles = cols // 128
    own_rows = first_moment.shape[0]
    pairs = own_rows // 2
    lines = own_rows * 2 * tiles

    message, own_factor = first_message(factor, weight, shards, reps)
    sent = lax.all_to_all(message, "fs", 0, 0, tiled=True)
    old_mine = sent[:, rows:]
    factor_mine = sent[:, :rows].reshape(-1, half)

    moments = lax.all_gather(jnp.concatenate([first_moment, second_moment], 0), "tp")
    moments = moments.reshape(2, 2, pairs, 2, tiles, 128)
    moments = moments.transpose(1, 3, 2, 0, 4, 5).reshape(2 * lines, 128)

    key_grad = key_gradient(query_two, key_two, values, out_grad, second_scale)
    key_both = lax.all_gather(key_grad, "tp", tiled=True)
    moments, key_both = lax.optimization_barrier((moments, key_both))

    sums = projected_sums(tokens_in, sent, key_both)
    arrived = lax.all_to_all(sums.reshape(shards, lines // 2, 128), "fs", 0, 0, tiled=True)
    part = lax.all_to_all(summed(arrived, 2 * reps), ("rep", "tp"), 0, 0, tiled=True)
    message, new_first, new_second = moments_step(
        part.reshape(reps * lines, 128), moments, shards
    )
    gathered = lax.all_to_all(message, "fs", 0, 0, tiled=True)

    old_all = jnp.zeros((shards, reps, *old_mine.shape[1:]), BF16)
    old_all = lax.dynamic_update_index_in_dim(old_all, old_mine, rep, 1)
    for i in (2, 1, 3):
        came = lax.ppermute(old_mine, "rep", [(j, (j + i) % reps) for j in range(reps)])
        old_all = lax.dynamic_update_index_in_dim(old_all, came, (rep + reps - i) % reps, 1)
    factor_other = lax.ppermute(factor_mine, "tp", [(0, 1), (1, 0)])

    copies, update_step, new_weight = new_weights(
        gathered.reshape(shards * lines, 128), sent, factor_other, old_all, own_factor, weight
    )

    def own_entries(value):
        value = value.reshape(2, pairs, 2, tiles * 128)
        value = jnp.where(core == 0, value[:, :, 0], value[:, :, 1])
        return jnp.stack([value[0], value[1]], axis=1).reshape(own_rows, cols)

    return (
        new_weight,
        copies.reshape(-1, cols),
        update_step,
        own_entries(new_first),
        own_entries(new_second),
    )


def solution(mesh):
    in_specs = (
        P(("fs", "rep"), None),
        P(("fs", "rep"), "tp"),
        P(("fs", "rep"), "tp"),
        P(("fs", "rep"), "tp"),
        P(("fs", "rep"), "tp"),
        P("tp"),
        P("fs", None),
        P("fs", "tp"),
        P("fs", "tp"),
        P("fs", "tp"),
    )
    out_specs = (P("fs", "tp"), P(None, "tp"), P("fs", "tp"), P("fs", "tp"), P("fs", "tp"))

    return jax.shard_map(
        on_device, mesh=mesh, in_specs=in_specs, out_specs=out_specs, check_vma=False
    )
```

time: 117 us -> 107 us (0.915)
  local copies, waits for them, and re-layouts: 5.02 us -> 12.3 us
  waiting for transfers between devices: 32.5 us -> 29 us
  Pallas kernels: 12.1 us -> 8.84 us
  other arithmetic: 3.84 us -> 0.75 us
  matrix products: 2.41 us -> 0 us
  blocking collectives: 5.76 us -> 3.99 us
  starting transfers between devices: 52.4 us -> 50.7 us
    unnamed x9 -> x20, local copies, waits for them, and re-layouts: 0.03 us -> 6.99 us
    all_to_all x4, waiting for transfers between devices: 32.3 us -> 28.9 us  [the longest x1 13 us: on_device(): gathered = lax.all_to_all(message, 'fs', 0, 0, tiled=True)]
    dynamic_update_slice x3, local copies, waits for them, and re-layouts: 0.13 us -> 2.98 us  [on_device(): lax.dynamic_update_index_in_dim(old_all, came, (rep + reps - i) % reps, 1)]
    dot_general x2 -> x0, matrix products: 2.41 us -> none  [dot32(): return jnp.dot(left, right, preferred_element_type=F32)]
    all_to_all x4, starting transfers between devices: 39.1 us -> 36.8 us  [the longest x1 16.7 us: on_device(): sent = lax.all_to_all(message, 'fs', 0, 0, tiled=True)]
    convert_element_type x3 -> x0, other arithmetic: 2.3 us -> none  [the longest x1 1.36 us: on_device(): (old_weight.astype(F32) - 0.1 * (dot32(factor_all, rows) * rate)).astype(...]
    pallas_call x1, Pallas kernels: 1.84 us -> 0.21 us  [first_message(): pl.pallas_call(first_message_body, out_shape=(jax.ShapeDtypeStruct((shard...]
    all_gather x1, blocking collectives: 3.81 us -> 2.18 us  [on_device(): key_both = lax.all_gather(key_grad, 'tp', tiled=True)]
  transfers between devices with their start and end apart: 8 -> 8, of which waited for: 4 -> 4; matrix products, arithmetic and copies ran while one was open for 4% -> 5% of each run, Pallas kernels for 6% -> 6%
where the time goes in v3:
time: 107 us; the launch traced here: 106 us
  starting transfers between devices  50.7 us (47%)
  waiting for transfers between devices  29 us (27%)
  local copies, waits for them, and re-layouts  12.3 us (11%)
  Pallas kernels  8.84 us (8%)
  blocking collectives  3.99 us (4%)
    all_to_all x1, starting transfers between devices, on_device(): sent = lax.all_to_all(message, 'fs', 0, 0, tiled=True)  16.7 us
    all_to_all x1, waiting for transfers between devices, on_device(): gathered = lax.all_to_all(message, 'fs', 0, 0, tiled=True)  13 us
    ppermute x3, starting transfers between devices, on_device(): lax.ppermute(old_mine, 'rep', [(j, (j + i) % reps) for j in range(reps)])  12 us
    all_to_all x1, waiting for transfers between devices, on_device(): sent = lax.all_to_all(message, 'fs', 0, 0, tiled=True)  11.2 us
    all_to_all x1, starting transfers between devices, on_device(): gathered = lax.all_to_all(message, 'fs', 0, 0, tiled=True)  10.2 us
    unnamed x20, local copies, waits for them, and re-layouts  6.99 us
    all_to_all x1, starting transfers between devices, on_device(): lax.all_to_all(sums.reshape(shards, lines // 2, 128), 'fs', 0, 0, tiled=T...  6.52 us
    pallas_call x1, Pallas kernels, key_gradient(): pl.pallas_call(key_gradient_body, out_shape=jax.ShapeDtypeStruct(query_ro...  3.43 us
  transfers between devices with their start and end apart: 8, of which 4 were waited for; matrix products, arithmetic and copies ran while one was open for 5% of the time, Pallas kernels for 6%

profile of v3, /device:TPU:8, one launch (start us, length us, event | category | flops | bytes accessed | tf_op | source)
XLA Modules:
  0.0 106.4 jit_solution(8908727917104866871)
XLA Ops:
  0.6 0.0 copy-start.6
  0.6 0.7 copy-done.6
  1.4 0.0 copy-start.8
  1.4 0.7 copy-done.8
  2.1 0.2 first_message.1
  2.3 0.0 copy-start.1
  2.3 0.9 copy-done.1
  3.2 0.0 copy-start
  3.2 16.7 %all-to-all-start = ((bf16[64,48,128]{2,1,0:T(8,128)(2,1)}), bf16[64,48,128]{2,1,0:T(8,128)(2,1)S(1)}, u32[]{:S(2)}, u32[]{:S(2)}) async-start(bf16[64,48,128]{2,1,0:T(8,128)(2,1)} %copy-done.1), calls=%async_computation | async-start | bytes 1572864 | tf_op jit(solution)/shard_map/all_to_all | solution.py:327
  19.9 0.7 pad_maximum_fusion
  20.6 1.8 %all-gather = f32[16,256]{1,0:T(8,128)S(1)} all-gather(f32[8,256]{1,0:T(8,128)S(1)} %pad_maximum_fusion), channel_id=2, replica_groups=mesh['fs'=64,'rep'=4,'tp'=2] {'tp'}, dimensions={0}, use_global_device_ids=true | all-gather | bytes 24576 | tf_op jit(solution)/shard_map/all_gather | solution.py:331
  22.5 0.0 copy-start.2
  22.5 1.0 copy-done.2
  23.5 1.0 copy-done.3
  24.6 0.9 copy-done.4
  25.5 0.9 copy-done.5
  26.5 0.7 copy-done.9
  27.1 3.4 %key_gradient.1 = bf16[512,256]{1,0:T(8,128)(2,1)S(1)} custom-call(f32[4]{0:T(128)S(1)} %copy-done.9, bf16[512,256]{1,0:T(8,128)(2,1)S(1)} %copy-done.4, bf16[512,256]{1,0:T(8,128)(2,1)S(1)} %copy-done.5, bf16[512,512]{1,0:T(8,128)(2,1)S(1)} %copy-done.2, bf16[512,512]{1,0:T(8,128)(2,1)S(1)} %copy-done.3), custom_call_target="tpu_custom_call" | custom-call | tf_op jit(solution)/shard_map/key_gradient/pallas_call | solution.py:70
  30.6 2.2 %all_gather.11.grad_ref = bf16[1024,256]{1,0:T(8,128)(2,1)S(1)} all-gather(bf16[512,256]{1,0:T(8,128)(2,1)S(1)} %key_gradient.1), channel_id=1, replica_groups=mesh['fs'=64,'rep'=4,'tp'=2] {'tp'}, dimensions={0}, use_global_device_ids=true | all-gather | bytes 786432 | tf_op jit(solution)/shard_map/all_gather | solution.py:336
  32.7 11.2 %all-to-all-done.sent_ref = bf16[64,48,128]{2,1,0:T(8,128)(2,1)S(1)} async-done(((bf16[64,48,128]{2,1,0:T(8,128)(2,1)}), bf16[64,48,128]{2,1,0:T(8,128)(2,1)S(1)}, u32[]{:S(2)}, u32[]{:S(2)}) %all-to-all-start) | async-done | bytes 786464 | tf_op jit(solution)/shard_map/all_to_all | solution.py:327
  43.9 0.7 slice.45
  44.6 4.9 %collective-permute-start.1 = (bf16[64,16,128]{2,1,0:T(8,128)(2,1)}, bf16[64,16,128]{2,1,0:T(8,128)(2,1)}, u32[]{:S(2)}, u32[]{:S(2)}) collective-permute-start(bf16[64,16,128]{2,1,0:T(8,128)(2,1)} %slice.45), channel_id=1, source_target_pairs={{0,4},{2,6},{4,0},{6,2},{1,5},{3,7},{5,1},{7,3},{8,12},{10,14},{12... | collective-permute-start | bytes 786440 | tf_op jit(solution)/shard_map/ppermute | solution.py:350
  49.6 0.0 copy-done
  49.6 1.9 %projected_sums.1 = bf16[512,128]{1,0:T(8,128)(2,1)} custom-call(bf16[512,2048]{1,0:T(8,128)(2,1)S(1)} %copy-done, bf16[64,48,128]{2,1,0:T(8,128)(2,1)S(1)} %all-to-all-done.sent_ref, bf16[1024,256]{1,0:T(8,128)(2,1)S(1)} %all_gather.11.grad_ref), custom_call_target="tpu_custom_call" | custom-call | flops 536870912 | bytes 2097152 | tf_op jit(solution)/shard_map/projected_sums/pallas_call | solution.py:147
  51.5 6.5 %all-to-all-start.1 = ((bf16[64,8,128]{2,1,0:T(8,128)(2,1)}), bf16[64,8,128]{2,1,0:T(8,128)(2,1)S(1)}, u32[]{:S(2)}, u32[]{:S(2)}) async-start(bf16[64,8,128]{2,1,0:T(8,128)(2,1)} %bitcast.2), calls=%async_computation.1 | async-start | bytes 262144 | tf_op jit(solution)/shard_map/all_to_all | solution.py:340
  58.0 2.5 %collective-permute-start.2 = (bf16[64,16,128]{2,1,0:T(8,128)(2,1)}, bf16[64,16,128]{2,1,0:T(8,128)(2,1)}, u32[]{:S(2)}, u32[]{:S(2)}) collective-permute-start(bf16[64,16,128]{2,1,0:T(8,128)(2,1)} %slice.45), channel_id=1, source_target_pairs={{0,2},{2,4},{4,6},{6,0},{1,3},{3,5},{5,7},{7,1},{8,10},{10,12},{12... | collective-permute-start | bytes 786440 | tf_op jit(solution)/shard_map/ppermute | solution.py:350
  60.5 4.6 %collective-permute-start.3 = (bf16[64,16,128]{2,1,0:T(8,128)(2,1)}, bf16[64,16,128]{2,1,0:T(8,128)(2,1)}, u32[]{:S(2)}, u32[]{:S(2)}) collective-permute-start(bf16[64,16,128]{2,1,0:T(8,128)(2,1)} %slice.45), channel_id=1, source_target_pairs={{0,6},{2,0},{4,2},{6,4},{1,7},{3,1},{5,3},{7,5},{8,14},{10,8},{12,... | collective-permute-start | bytes 786440 | tf_op jit(solution)/shard_map/ppermute | solution.py:350
  65.1 0.0 copy-start.7
  65.2 1.9 %collective-permute-start = (bf16[2048,128]{1,0:T(8,128)(2,1)S(1)}, bf16[2048,128]{1,0:T(8,128)(2,1)S(1)}, u32[]{:S(2)}, u32[]{:S(2)}) collective-permute-start(bf16[2048,128]{1,0:T(8,128)(2,1)S(1)} %bitcast.33), channel_id=1, source_target_pairs={{0,1},{1,0},{2,3},{3,2},{4,5},{5,4},{6,7},{7,6},{8,9},{9,8},{10,11... | collective-permute-start | bytes 1572872 | tf_op jit(solution)/shard_map/ppermute | solution.py:352
  67.1 0.2 broadcast_in_dim.16
  67.4 2.5 %all-to-all-done.1.arrived_ref = bf16[64,8,128]{2,1,0:T(8,128)(2,1)S(1)} async-done(((bf16[64,8,128]{2,1,0:T(8,128)(2,1)}), bf16[64,8,128]{2,1,0:T(8,128)(2,1)S(1)}, u32[]{:S(2)}, u32[]{:S(2)}) %all-to-all-start.1) | async-done | bytes 131104 | tf_op jit(solution)/shard_map/all_to_all | solution.py:340
  69.9 0.7 summed.1
  70.6 3.3 %all-to-all-start.2 = ((f32[8,8,128]{2,1,0:T(8,128)}), f32[8,8,128]{2,1,0:T(8,128)S(1)}, u32[]{:S(2)}, u32[]{:S(2)}) async-start(f32[8,8,128]{2,1,0:T(8,128)} %summed.1), calls=%async_computation.2 | async-start | bytes 65536 | tf_op jit(solution)/shard_map/all_to_all | solution.py:341
  73.9 0.0 collective-permute-done.1
  73.9 1.0 bitcast_dynamic-update-slice_fusion.1
  74.9 0.0 collective-permute-done.2
  74.9 1.0 bitcast_dynamic-update-slice_fusion
  76.0 0.0 collective-permute-done.3
  76.0 1.0 bitcast_dynamic-update-slice_fusion.3.old_ref
  77.0 2.3 %all-to-all-done.2 = f32[8,8,128]{2,1,0:T(8,128)S(1)} async-done(((f32[8,8,128]{2,1,0:T(8,128)}), f32[8,8,128]{2,1,0:T(8,128)S(1)}, u32[]{:S(2)}, u32[]{:S(2)}) %all-to-all-start.2) | async-done | bytes 32800 | tf_op jit(solution)/shard_map/all_to_all | solution.py:341
  79.3 0.8 moments_step.1
  80.1 10.2 %all-to-all-start.3 = ((bf16[64,16,128]{2,1,0:T(8,128)(2,1)}), bf16[64,16,128]{2,1,0:T(8,128)(2,1)S(1)}, u32[]{:S(2)}, u32[]{:S(2)}) async-start(bf16[64,16,128]{2,1,0:T(8,128)(2,1)} %get-tuple-element.18), calls=%async_computation.3 | async-start | bytes 524288 | tf_op jit(solution)/shard_map/all_to_all | solution.py:345
  90.4 0.6 reshape.63
  91.0 0.6 reshape.65
  91.7 0.0 collective-permute-done.swapped_ref
  91.7 13.0 %all-to-all-done.3 = bf16[64,16,128]{2,1,0:T(8,128)(2,1)S(1)} async-done(((bf16[64,16,128]{2,1,0:T(8,128)(2,1)}), bf16[64,16,128]{2,1,0:T(8,128)(2,1)S(1)}, u32[]{:S(2)}, u32[]{:S(2)}) %all-to-all-start.3) | async-done | bytes 262176 | tf_op jit(solution)/shard_map/all_to_all | solution.py:345
  104.6 0.0 copy-done.7
  104.6 1.8 %new_weights.1 = (bf16[64,4,8,256]{3,2,1,0:T(8,128)(2,1)}, f32[32,256]{1,0:T(8,128)}, f32[32,256]{1,0:T(8,128)}) custom-call(bf16[1024,128]{1,0:T(8,128)(2,1)S(1)} %bitcast.30, bf16[64,48,128]{2,1,0:T(8,128)(2,1)S(1)} %all-to-all-done.sent_ref, bf16[2048,128]{1,0:T(8,128)(2,1)S(1)} %collective-permute-done.swapped_ref, ...), custom_call_target="tpu_custom_call" | custom-call | flops 268435456 | bytes 2097152 | tf_op jit(solution)/shard_map/new_weights/pallas_call | solution.py:285
  (15 shorter events, 0.2 us)
Async XLA Ops:
  0.6 0.8 copy-start.6
  1.4 0.7 copy-start.8
  2.3 0.9 copy-start.1
  3.2 46.3 %copy-start = (bf16[512,2048]{1,0:T(8,128)(2,1)S(1)}, bf16[512,2048]{1,0:T(8,128)(2,1)}, u32[]{:S(2)}) copy-start(bf16[512,2048]{1,0:T(8,128)(2,1)} %tokens_ref.1) | copy-start | bytes 6291460
  3.2 40.7 %all-to-all-start = ((bf16[64,48,128]{2,1,0:T(8,128)(2,1)}), bf16[64,48,128]{2,1,0:T(8,128)(2,1)S(1)}, u32[]{:S(2)}, u32[]{:S(2)}) async-start(bf16[64,48,128]{2,1,0:T(8,128)(2,1)} %copy-done.1), calls=%async_computation | async-start | bytes 1572864 | tf_op jit(solution)/shard_map/all_to_all | solution.py:327
  22.5 1.0 copy-start.2
  23.5 1.0 copy-start.3
  24.6 0.9 copy-start.4
  25.5 0.9 copy-start.5
  26.5 0.7 copy-start.9
  44.6 29.3 %collective-permute-start.1 = (bf16[64,16,128]{2,1,0:T(8,128)(2,1)}, bf16[64,16,128]{2,1,0:T(8,128)(2,1)}, u32[]{:S(2)}, u32[]{:S(2)}) collective-permute-start(bf16[64,16,128]{2,1,0:T(8,128)(2,1)} %slice.45), channel_id=1, source_target_pairs={{0,4},{2,6},{4,0},{6,2},{1,5},{3,7},{5,1},{7,3},{8,12},{10,14},{12... | collective-permute-start | bytes 786440 | tf_op jit(solution)/shard_map/ppermute | solution.py:350
  51.5 18.4 %all-to-all-start.1 = ((bf16[64,8,128]{2,1,0:T(8,128)(2,1)}), bf16[64,8,128]{2,1,0:T(8,128)(2,1)S(1)}, u32[]{:S(2)}, u32[]{:S(2)}) async-start(bf16[64,8,128]{2,1,0:T(8,128)(2,1)} %bitcast.2), calls=%async_computation.1 | async-start | bytes 262144 | tf_op jit(solution)/shard_map/all_to_all | solution.py:340
  58.0 16.9 %collective-permute-start.2 = (bf16[64,16,128]{2,1,0:T(8,128)(2,1)}, bf16[64,16,128]{2,1,0:T(8,128)(2,1)}, u32[]{:S(2)}, u32[]{:S(2)}) collective-permute-start(bf16[64,16,128]{2,1,0:T(8,128)(2,1)} %slice.45), channel_id=1, source_target_pairs={{0,2},{2,4},{4,6},{6,0},{1,3},{3,5},{5,7},{7,1},{8,10},{10,12},{12... | collective-permute-start | bytes 786440 | tf_op jit(solution)/shard_map/ppermute | solution.py:350
  60.5 15.4 %collective-permute-start.3 = (bf16[64,16,128]{2,1,0:T(8,128)(2,1)}, bf16[64,16,128]{2,1,0:T(8,128)(2,1)}, u32[]{:S(2)}, u32[]{:S(2)}) collective-permute-start(bf16[64,16,128]{2,1,0:T(8,128)(2,1)} %slice.45), channel_id=1, source_target_pairs={{0,6},{2,0},{4,2},{6,4},{1,7},{3,1},{5,3},{7,5},{8,14},{10,8},{12,... | collective-permute-start | bytes 786440 | tf_op jit(solution)/shard_map/ppermute | solution.py:350
  65.1 39.5 %copy-start.7 = (f32[32,256]{1,0:T(8,128)S(1)}, f32[32,256]{1,0:T(8,128)}, u32[]{:S(2)}) copy-start(f32[32,256]{1,0:T(8,128)} %weight_ref.3) | copy-start | bytes 98308
  65.2 26.5 %collective-permute-start = (bf16[2048,128]{1,0:T(8,128)(2,1)S(1)}, bf16[2048,128]{1,0:T(8,128)(2,1)S(1)}, u32[]{:S(2)}, u32[]{:S(2)}) collective-permute-start(bf16[2048,128]{1,0:T(8,128)(2,1)S(1)} %bitcast.33), channel_id=1, source_target_pairs={{0,1},{1,0},{2,3},{3,2},{4,5},{5,4},{6,7},{7,6},{8,9},{9,8},{10,11... | collective-permute-start | bytes 1572872 | tf_op jit(solution)/shard_map/ppermute | solution.py:352
  70.6 8.7 %all-to-all-start.2 = ((f32[8,8,128]{2,1,0:T(8,128)}), f32[8,8,128]{2,1,0:T(8,128)S(1)}, u32[]{:S(2)}, u32[]{:S(2)}) async-start(f32[8,8,128]{2,1,0:T(8,128)} %summed.1), calls=%async_computation.2 | async-start | bytes 65536 | tf_op jit(solution)/shard_map/all_to_all | solution.py:341
  80.1 24.5 %all-to-all-start.3 = ((bf16[64,16,128]{2,1,0:T(8,128)(2,1)}), bf16[64,16,128]{2,1,0:T(8,128)(2,1)S(1)}, u32[]{:S(2)}, u32[]{:S(2)}) async-start(bf16[64,16,128]{2,1,0:T(8,128)(2,1)} %get-tuple-element.18), calls=%async_computation.3 | async-start | bytes 524288 | tf_op jit(solution)/shard_map/all_to_all | solution.py:345

commit v4 on v3

--- a/solution.py
+++ b/solution.py
@@ -77,43 +77,64 @@
     )(second_scale, query_rows, key_rows, value_rows, grad_rows)
 
 
-def first_message_body(factor_ref, weight_ref, out_ref, own_ref):
+def first_message_body(
+    factor_hbm, weight_hbm, out_hbm, own_ref, factor_ref, weight_ref, out_ref, sems
+):
     shards = out_ref.shape[0]
     rows, rank = factor_ref.shape
     half = rank // 2
-    share = (out_ref.shape[1] - rows) // 2
+    share = weight_ref.shape[0]
+    start = pl.multiple_of(lax.axis_index("rep") * share, share)
+    factor_copy = pltpu.make_async_copy(factor_hbm, factor_ref, sems.at[0])
+    weight_copy = pltpu.make_async_copy(weight_hbm.at[pl.ds(start, share), :], weight_ref, sems.at[1])
+    factor_copy.start()
+    weight_copy.start()
     core = lax.axis_index("tp")
     ranks = lax.broadcasted_iota(jnp.int32, (rank, half), 0)
     places = lax.broadcasted_iota(jnp.int32, (rank, half), 1)
     pair = sum((places >= i * shards).astype(jnp.int32) for i in range(1, half // shards))
     wanted = (places - pair * shards) * (rank // shards) + 2 * pair
+    pick = (ranks == wanted + core).astype(F32).astype(BF16)
+    pick_other = (ranks == wanted + 1 - core).astype(F32).astype(BF16)
+    factor_copy.wait()
     factor = factor_ref[...]
-    mine = dot32(factor, (ranks == wanted + core).astype(F32).astype(BF16)).astype(BF16)
-    other = dot32(factor, (ranks == wanted + 1 - core).astype(F32).astype(BF16)).astype(BF16)
+    mine = dot32(factor, pick).astype(BF16)
     own_ref[:, :half] = mine
-    own_ref[:, half:] = other
-    start = pl.multiple_of(lax.axis_index("rep") * share, share)
-    old = weight_ref[pl.ds(start, share), :].astype(BF16)
+    own_ref[:, half:] = dot32(factor, pick_other).astype(BF16)
     out_ref[:, :rows, :] = jnp.broadcast_to(mine[None], (shards, rows, half))
+    weight_copy.wait()
+    old = weight_ref[...].astype(BF16)
     for i in range(2):
         piece = old[:, i * half : i * half + half]
         out_ref[:, rows + i * share : rows + i * share + share, :] = jnp.broadcast_to(
             piece[None], (shards, share, half)
         )
+    out_copy = pltpu.make_async_copy(out_ref, out_hbm, sems.at[0])
+    out_copy.start()
+    out_copy.wait()
 
 
 def first_message(factor, weight, shards, reps):
     rows, rank = factor.shape
     half = rank // 2
+    share = rows // reps
+    message = (shards, rows + 2 * share, half)
+    any_spec = pl.BlockSpec(memory_space=pltpu.HBM)
     return pl.pallas_call(
         first_message_body,
         out_shape=(
-            jax.ShapeDtypeStruct((shards, rows + 2 * (rows // reps), half), BF16),
+            jax.ShapeDtypeStruct(message, BF16),
             jax.ShapeDtypeStruct((rows, rank), BF16),
         ),
-        in_specs=2 * [VMEM_SPEC],
-        out_specs=(VMEM_SPEC, VMEM_SPEC),
-        compiler_params=pltpu.CompilerParams(vmem_limit_bytes=8 * MIB),
+        in_specs=2 * [any_spec],
+        out_specs=(any_spec, VMEM_SPEC),
+        scratch_shapes=[
+            pltpu.VMEM((rows, rank), BF16),
+            pltpu.VMEM((share, weight.shape[1]), F32),
+            pltpu.VMEM(message, BF16),
+            pltpu.SemaphoreType.DMA((2,)),
+        ],
+        compiler_params=pltpu.CompilerParams(vmem_limit_bytes=60 * MIB),
         name="first_message",
     )(factor, weight)
 
@@ -175,7 +196,6 @@
 
 
 def moments_step_body(part_ref, moments_ref, message_ref, first_ref, second_ref):
-    shards = message_ref.shape[0]
     lines = first_ref.shape[0]
     core = lax.axis_index("tp")
     total = part_ref[:lines, :]
@@ -188,26 +208,30 @@
     direction = (new_first / (jnp.sqrt(new_second) + 1e-08)).astype(BF16).astype(F32)
     squares = direction * direction
     squares = jnp.sum(jnp.sum(squares, axis=1, keepdims=True), axis=0, keepdims=True)
-    quarter = lines // 8
     own = []
-    for i in range(4):
-        base = i * 2 * quarter
-        own.append(
-            jnp.where(
-                core == 0,
-                direction[base : base + quarter],
-                direction[base + quarter : base + 2 * quarter],
-            )
-        )
+    tiles = lines // 8
+    for pair in range(2):
+        made = []
+        for parity in range(2):
+            base = (parity * 2 + pair) * 2 * tiles
+            for tile in range(tiles):
+                made.append(
+                    jnp.where(
+                        core == 0,
+                        direction[base + tile : base + tile + 1],
+                        direction[base + tiles + tile : base + tiles + tile + 1],
+                    )
+                )
+        own.append(jnp.concatenate(made, axis=1))
     high = squares.astype(BF16).astype(F32)
     middle = (squares - high).astype(BF16).astype(F32)
     low = squares - high - middle
-    lane = lax.broadcasted_iota(jnp.int32, (lines // 2, 128), 1)
-    row = lax.broadcasted_iota(jnp.int32, (lines // 2, 128), 0)
+    lane = lax.broadcasted_iota(jnp.int32, (1, 128), 1)
     packed = jnp.where(lane == 0, high, jnp.where(lane == 1, middle, jnp.where(lane == 2, low, 0.0)))
-    own.append(jnp.where(row == 0, packed, 0.0))
+    own[0] = jnp.concatenate([own[0], packed], axis=1)
+    own[1] = jnp.concatenate([own[1], jnp.zeros_like(packed)], axis=1)
     message = jnp.concatenate(own, axis=0).astype(BF16)
-    message_ref[...] = jnp.broadcast_to(message[None], (shards, lines, 128))
+    message_ref[...] = jnp.broadcast_to(message[None], message_ref.shape)
 
 
 def moments_step(part, moments, shards):
@@ -215,7 +239,7 @@
     return pl.pallas_call(
         moments_step_body,
         out_shape=(
-            jax.ShapeDtypeStruct((shards, lines, 128), BF16),
+            jax.ShapeDtypeStruct((shards, 2, lines * 32 + 128), BF16),
             jax.ShapeDtypeStruct((lines, 128), F32),
             jax.ShapeDtypeStruct((lines, 128), F32),
         ),
@@ -228,10 +252,9 @@
 
 def new_weights_body(
     gathered_ref, sent_ref, swapped_ref, old_ref, own_ref, weight_ref,
-    copies_ref, update_ref, weight_out_ref, laid_ref,
+    copies_ref, update_ref, weight_out_ref,
 ):
     shards = sent_ref.shape[0]
-    lines = gathered_ref.shape[0] // shards
     width, half = swapped_ref.shape
     rows = width // shards
     reps, share = copies_ref.shape[1:3]
@@ -239,16 +262,15 @@
     tiles = cols // 128
     pairs = half // shards
     core = lax.axis_index("tp")
-    laid_ref[...] = gathered_ref[...].astype(F32)
-
-    def line(place):
-        return laid_ref[pl.ds(place, shards, lines), :]
+
+    def line(pair, place):
+        return gathered_ref[:, pair, place * 128 : place * 128 + 128].astype(F32)
 
     def directions(parity):
         return jnp.concatenate(
             [
                 jnp.concatenate(
-                    [line((parity * pairs + pair) * tiles + tile) for tile in range(tiles)], axis=1
+                    [line(pair, parity * tiles + tile) for tile in range(tiles)], axis=1
                 )
                 for pair in range(pairs)
             ],
@@ -258,25 +280,31 @@
     even, odd = directions(0), directions(1)
     mine = jnp.where(core == 0, even, odd).astype(BF16)
     other = jnp.where(core == 0, odd, even).astype(BF16)
-    squares = line(lines // 2)
+    squares = line(0, 2 * tiles)
     squares = jnp.sum(jnp.sum(squares, axis=1, keepdims=True), axis=0, keepdims=True)
     rate = lax.rsqrt(squares / (RANK * KW) + 1e-06)
-    update = (dot32(own_ref[:, :half], mine) + dot32(own_ref[:, half:], other)) * rate
-    update_ref[...] = update
-    weight_out_ref[...] = weight_ref[...] - 0.1 * update
+    both = jnp.concatenate([mine, other], axis=0)
     pieces = 4
     group = shards // pieces
     for piece in range(pieces):
         owners = slice(piece * group, piece * group + group)
-        factor = sent_ref[owners, :rows, :].reshape(group * rows, half)
-        swapped = swapped_ref[piece * group * rows : (piece + 1) * group * rows, :]
-        step = (dot32(factor, mine) + dot32(swapped, other)) * (0.1 * rate)
+        factor = jnp.concatenate(
+            [
+                sent_ref[owners, :rows, :].reshape(group * rows, half),
+                swapped_ref[piece * group * rows : (piece + 1) * group * rows, :],
+            ],
+            axis=1,
+        )
+        step = dot32(factor, both) * (0.1 * rate)
         for i in range(cols // half):
             lanes = slice(i * half, i * half + half)
             old = old_ref[owners, :, i * share : i * share + share, :].astype(F32)
             copies_ref[owners, :, :, lanes] = (
                 old - step[:, lanes].reshape(group, reps, share, half)
             ).astype(BF16)
+    update = dot32(own_ref[...], both) * rate
+    update_ref[...] = update
+    weight_out_ref[...] = weight_ref[...] - 0.1 * update
 
 
 def new_weights(gathered, sent, swapped, old, own_factor, weight):
@@ -291,7 +319,6 @@
         ),
         in_specs=6 * [VMEM_SPEC],
         out_specs=3 * (VMEM_SPEC,),
-        scratch_shapes=[pltpu.VMEM(gathered.shape, F32)],
         cost_estimate=pl.CostEstimate(
             flops=4 * swapped.size * cols, bytes_accessed=8 * swapped.size, transcendentals=0
         ),
@@ -352,7 +379,7 @@
     factor_other = lax.ppermute(factor_mine, "tp", [(0, 1), (1, 0)])
 
     copies, update_step, new_weight = new_weights(
-        gathered.reshape(shards * lines, 128), sent, factor_other, old_all, own_factor, weight
+        gathered, sent, factor_other, old_all, own_factor, weight
     )
 
     def own_entries(value):

time: 107 us -> 105 us (0.981)
  local copies, waits for them, and re-layouts: 12.3 us -> 8.99 us
  Pallas kernels: 8.84 us -> 10.9 us
    unnamed x20 -> x16, local copies, waits for them, and re-layouts: 6.99 us -> 4.65 us
    pallas_call x1, Pallas kernels: 0.21 us -> 2.41 us  [first_message(): pl.pallas_call(first_message_body, out_shape=(jax.ShapeDtypeStruct(messag...]
    all_to_all x1, waiting for transfers between devices: 13 us -> 11.1 us  [on_device(): gathered = lax.all_to_all(message, 'fs', 0, 0, tiled=True)]
  transfers between devices with their start and end apart: 8 -> 8, of which waited for: 4 -> 4; matrix products, arithmetic and copies ran while one was open for 5% -> 4% of each run, Pallas kernels for 6% -> 7%
where the time goes in v4:
time: 105 us; the launch traced here: 104 us
  starting transfers between devices  50.7 us (48%)
  waiting for transfers between devices  28.1 us (27%)
  Pallas kernels  10.9 us (10%)
  local copies, waits for them, and re-layouts  8.99 us (9%)
  blocking collectives  3.99 us (4%)
    all_to_all x1, starting transfers between devices, on_device(): sent = lax.all_to_all(message, 'fs', 0, 0, tiled=True)  16.7 us
    ppermute x3, starting transfers between devices, on_device(): lax.ppermute(old_mine, 'rep', [(j, (j + i) % reps) for j in range(reps)])  12 us
    all_to_all x1, waiting for transfers between devices, on_device(): sent = lax.all_to_all(message, 'fs', 0, 0, tiled=True)  11.2 us
    all_to_all x1, waiting for transfers between devices, on_device(): gathered = lax.all_to_all(message, 'fs', 0, 0, tiled=True)  11.1 us
    all_to_all x1, starting transfers between devices, on_device(): gathered = lax.all_to_all(message, 'fs', 0, 0, tiled=True)  10.2 us
    all_to_all x1, starting transfers between devices, on_device(): lax.all_to_all(sums.reshape(shards, lines // 2, 128), 'fs', 0, 0, tiled=T...  6.52 us
    unnamed x16, local copies, waits for them, and re-layouts  4.65 us
    pallas_call x1, Pallas kernels, key_gradient(): pl.pallas_call(key_gradient_body, out_shape=jax.ShapeDtypeStruct(query_ro...  3.43 us
  transfers between devices with their start and end apart: 8, of which 4 were waited for; matrix products, arithmetic and copies ran while one was open for 4% of the time, Pallas kernels for 7%

profile of v4, /device:TPU:8, one launch (start us, length us, event | category | flops | bytes accessed | tf_op | source)
XLA Modules:
  0.0 104.3 jit_solution(3326901204057054208)
XLA Ops:
  0.6 2.4 %first_message.1 = (bf16[64,48,128]{2,1,0:T(8,128)(2,1)}, bf16[32,256]{1,0:T(8,128)(2,1)}) custom-call(bf16[32,256]{1,0:T(8,128)(2,1)} %factor_hbm.1, f32[32,256]{1,0:T(8,128)} %weight_ref.1), custom_call_target="tpu_custom_call" | custom-call | tf_op jit(solution)/shard_map/first_message/pallas_call | solution.py:123
  3.1 0.0 copy-start
  3.1 16.7 %all-to-all-start = ((bf16[64,48,128]{2,1,0:T(8,128)(2,1)}), bf16[64,48,128]{2,1,0:T(8,128)(2,1)S(1)}, u32[]{:S(2)}, u32[]{:S(2)}) async-start(bf16[64,48,128]{2,1,0:T(8,128)(2,1)} %get-tuple-element.15), calls=%async_computation | async-start | bytes 1572864 | tf_op jit(solution)/shard_map/all_to_all | solution.py:354
  19.8 0.7 pad_maximum_fusion
  20.5 1.8 %all-gather = f32[16,256]{1,0:T(8,128)S(1)} all-gather(f32[8,256]{1,0:T(8,128)S(1)} %pad_maximum_fusion), channel_id=2, replica_groups=mesh['fs'=64,'rep'=4,'tp'=2] {'tp'}, dimensions={0}, use_global_device_ids=true | all-gather | bytes 24576 | tf_op jit(solution)/shard_map/all_gather | solution.py:358
  22.3 0.0 copy-start.1
  22.4 1.0 copy-done.1
  23.4 0.0 copy-start.2
  23.4 1.0 copy-done.2
  24.4 0.0 copy-start.3
  24.4 0.9 copy-done.3
  25.4 0.0 copy-start.4
  25.4 0.9 copy-done.4
  26.3 0.0 copy-start.7
  26.3 0.7 copy-done.7
  27.0 3.4 %key_gradient.1 = bf16[512,256]{1,0:T(8,128)(2,1)S(1)} custom-call(f32[4]{0:T(128)S(1)} %copy-done.7, bf16[512,256]{1,0:T(8,128)(2,1)S(1)} %copy-done.3, bf16[512,256]{1,0:T(8,128)(2,1)S(1)} %copy-done.4, bf16[512,512]{1,0:T(8,128)(2,1)S(1)} %copy-done.1, bf16[512,512]{1,0:T(8,128)(2,1)S(1)} %copy-done.2), custom_call_target="tpu_custom_call" | custom-call | tf_op jit(solution)/shard_map/key_gradient/pallas_call | solution.py:70
  30.4 2.2 %all_gather.11.grad_ref = bf16[1024,256]{1,0:T(8,128)(2,1)S(1)} all-gather(bf16[512,256]{1,0:T(8,128)(2,1)S(1)} %key_gradient.1), channel_id=1, replica_groups=mesh['fs'=64,'rep'=4,'tp'=2] {'tp'}, dimensions={0}, use_global_device_ids=true | all-gather | bytes 786432 | tf_op jit(solution)/shard_map/all_gather | solution.py:363
  32.6 11.2 %all-to-all-done.sent_ref = bf16[64,48,128]{2,1,0:T(8,128)(2,1)S(1)} async-done(((bf16[64,48,128]{2,1,0:T(8,128)(2,1)}), bf16[64,48,128]{2,1,0:T(8,128)(2,1)S(1)}, u32[]{:S(2)}, u32[]{:S(2)}) %all-to-all-start) | async-done | bytes 786464 | tf_op jit(solution)/shard_map/all_to_all | solution.py:354
  43.8 0.7 slice.45
  44.5 4.9 %collective-permute-start.1 = (bf16[64,16,128]{2,1,0:T(8,128)(2,1)}, bf16[64,16,128]{2,1,0:T(8,128)(2,1)}, u32[]{:S(2)}, u32[]{:S(2)}) collective-permute-start(bf16[64,16,128]{2,1,0:T(8,128)(2,1)} %slice.45), channel_id=1, source_target_pairs={{0,4},{2,6},{4,0},{6,2},{1,5},{3,7},{5,1},{7,3},{8,12},{10,14},{12... | collective-permute-start | bytes 786440 | tf_op jit(solution)/shard_map/ppermute | solution.py:377
  49.4 0.0 copy-done
  49.4 1.9 %projected_sums.1 = bf16[512,128]{1,0:T(8,128)(2,1)} custom-call(bf16[512,2048]{1,0:T(8,128)(2,1)S(1)} %copy-done, bf16[64,48,128]{2,1,0:T(8,128)(2,1)S(1)} %all-to-all-done.sent_ref, bf16[1024,256]{1,0:T(8,128)(2,1)S(1)} %all_gather.11.grad_ref), custom_call_target="tpu_custom_call" | custom-call | flops 536870912 | bytes 2097152 | tf_op jit(solution)/shard_map/projected_sums/pallas_call | solution.py:168
  51.3 6.5 %all-to-all-start.1 = ((bf16[64,8,128]{2,1,0:T(8,128)(2,1)}), bf16[64,8,128]{2,1,0:T(8,128)(2,1)S(1)}, u32[]{:S(2)}, u32[]{:S(2)}) async-start(bf16[64,8,128]{2,1,0:T(8,128)(2,1)} %bitcast.2), calls=%async_computation.1 | async-start | bytes 262144 | tf_op jit(solution)/shard_map/all_to_all | solution.py:367
  57.9 2.5 %collective-permute-start.2 = (bf16[64,16,128]{2,1,0:T(8,128)(2,1)}, bf16[64,16,128]{2,1,0:T(8,128)(2,1)}, u32[]{:S(2)}, u32[]{:S(2)}) collective-permute-start(bf16[64,16,128]{2,1,0:T(8,128)(2,1)} %slice.45), channel_id=1, source_target_pairs={{0,2},{2,4},{4,6},{6,0},{1,3},{3,5},{5,7},{7,1},{8,10},{10,12},{12... | collective-permute-start | bytes 786440 | tf_op jit(solution)/shard_map/ppermute | solution.py:377
  60.4 4.6 %collective-permute-start.3 = (bf16[64,16,128]{2,1,0:T(8,128)(2,1)}, bf16[64,16,128]{2,1,0:T(8,128)(2,1)S(1)}, u32[]{:S(2)}, u32[]{:S(2)}) collective-permute-start(bf16[64,16,128]{2,1,0:T(8,128)(2,1)} %slice.45), channel_id=1, source_target_pairs={{0,6},{2,0},{4,2},{6,4},{1,7},{3,1},{5,3},{7,5},{8,14},{10,8},{12,... | collective-permute-start | bytes 786440 | tf_op jit(solution)/shard_map/ppermute | solution.py:377
  65.0 0.0 copy-start.5
  65.0 0.0 copy-start.6
  65.1 1.9 %collective-permute-start = (bf16[2048,128]{1,0:T(8,128)(2,1)S(1)}, bf16[2048,128]{1,0:T(8,128)(2,1)S(1)}, u32[]{:S(2)}, u32[]{:S(2)}) collective-permute-start(bf16[2048,128]{1,0:T(8,128)(2,1)S(1)} %bitcast.31), channel_id=1, source_target_pairs={{0,1},{1,0},{2,3},{3,2},{4,5},{5,4},{6,7},{7,6},{8,9},{9,8},{10,11... | collective-permute-start | bytes 1572872 | tf_op jit(solution)/shard_map/ppermute | solution.py:379
  67.0 0.2 broadcast_in_dim.16
  67.3 2.5 %all-to-all-done.1.arrived_ref = bf16[64,8,128]{2,1,0:T(8,128)(2,1)S(1)} async-done(((bf16[64,8,128]{2,1,0:T(8,128)(2,1)}), bf16[64,8,128]{2,1,0:T(8,128)(2,1)S(1)}, u32[]{:S(2)}, u32[]{:S(2)}) %all-to-all-start.1) | async-done | bytes 131104 | tf_op jit(solution)/shard_map/all_to_all | solution.py:367
  69.8 0.7 summed.1
  70.5 3.3 %all-to-all-start.2 = ((f32[8,8,128]{2,1,0:T(8,128)}), f32[8,8,128]{2,1,0:T(8,128)S(1)}, u32[]{:S(2)}, u32[]{:S(2)}) async-start(f32[8,8,128]{2,1,0:T(8,128)} %summed.1), calls=%async_computation.2 | async-start | bytes 65536 | tf_op jit(solution)/shard_map/all_to_all | solution.py:368
  73.8 0.0 collective-permute-done.1
  73.8 1.0 bitcast_dynamic-update-slice_fusion.1
  74.8 0.0 collective-permute-done.2
  74.8 1.0 bitcast_dynamic-update-slice_fusion
  75.8 0.0 collective-permute-done.3
  75.9 3.3 %all-to-all-done.2 = f32[8,8,128]{2,1,0:T(8,128)S(1)} async-done(((f32[8,8,128]{2,1,0:T(8,128)}), f32[8,8,128]{2,1,0:T(8,128)S(1)}, u32[]{:S(2)}, u32[]{:S(2)}) %all-to-all-start.2) | async-done | bytes 32800 | tf_op jit(solution)/shard_map/all_to_all | solution.py:368
  79.2 0.8 moments_step.1
  80.0 10.2 %all-to-all-start.3 = ((bf16[64,2,640]{2,1,0:T(2,128)(2,1)}), bf16[64,2,640]{2,1,0:T(2,128)(2,1)S(1)}, u32[]{:S(2)}, u32[]{:S(2)}) async-start(bf16[64,2,640]{2,1,0:T(2,128)(2,1)} %get-tuple-element.18), calls=%async_computation.3 | async-start | bytes 327680 | tf_op jit(solution)/shard_map/all_to_all | solution.py:372
  90.3 0.6 reshape.59
  90.9 0.6 reshape.61
  91.5 0.0 collective-permute-done.swapped_ref
  91.5 11.1 %all-to-all-done.3.gathered_ref = bf16[64,2,640]{2,1,0:T(2,128)(2,1)S(1)} async-done(((bf16[64,2,640]{2,1,0:T(2,128)(2,1)}), bf16[64,2,640]{2,1,0:T(2,128)(2,1)S(1)}, u32[]{:S(2)}, u32[]{:S(2)}) %all-to-all-start.3) | async-done | bytes 163872 | tf_op jit(solution)/shard_map/all_to_all | solution.py:372
  102.6 0.0 copy-done.5
  102.6 0.0 copy-done.6
  102.6 1.7 %new_weights.1 = (bf16[64,4,8,256]{3,2,1,0:T(8,128)(2,1)}, f32[32,256]{1,0:T(8,128)}, f32[32,256]{1,0:T(8,128)}) custom-call(bf16[64,2,640]{2,1,0:T(2,128)(2,1)S(1)} %all-to-all-done.3.gathered_ref, bf16[64,48,128]{2,1,0:T(8,128)(2,1)S(1)} %all-to-all-done.sent_ref, bf16[2048,128]{1,0:T(8,128)(2,1)S(1)} %collective-permute-done.swapped_ref, ...), custom_call_target="tpu_custom_call" | custom-call | flops 268435456 | bytes 2097152 | tf_op jit(solution)/shard_map/new_weights/pallas_call | solution.py:313
  (12 shorter events, 0.2 us)
Async XLA Ops:
  3.1 46.4 %copy-start = (bf16[512,2048]{1,0:T(8,128)(2,1)S(1)}, bf16[512,2048]{1,0:T(8,128)(2,1)}, u32[]{:S(2)}) copy-start(bf16[512,2048]{1,0:T(8,128)(2,1)} %tokens_ref.1) | copy-start | bytes 6291460
  3.1 40.7 %all-to-all-start = ((bf16[64,48,128]{2,1,0:T(8,128)(2,1)}), bf16[64,48,128]{2,1,0:T(8,128)(2,1)S(1)}, u32[]{:S(2)}, u32[]{:S(2)}) async-start(bf16[64,48,128]{2,1,0:T(8,128)(2,1)} %get-tuple-element.15), calls=%async_computation | async-start | bytes 1572864 | tf_op jit(solution)/shard_map/all_to_all | solution.py:354
  22.3 1.0 %copy-start.1 = (bf16[512,512]{1,0:T(8,128)(2,1)S(1)}, bf16[512,512]{1,0:T(8,128)(2,1)}, u32[]{:S(2)}) copy-start(bf16[512,512]{1,0:T(8,128)(2,1)} %value_ref.1) | copy-start | bytes 1572868
  23.4 1.0 copy-start.2
  24.4 0.9 copy-start.3
  25.4 0.9 copy-start.4
  26.3 0.7 copy-start.7
  44.5 29.3 %collective-permute-start.1 = (bf16[64,16,128]{2,1,0:T(8,128)(2,1)}, bf16[64,16,128]{2,1,0:T(8,128)(2,1)}, u32[]{:S(2)}, u32[]{:S(2)}) collective-permute-start(bf16[64,16,128]{2,1,0:T(8,128)(2,1)} %slice.45), channel_id=1, source_target_pairs={{0,4},{2,6},{4,0},{6,2},{1,5},{3,7},{5,1},{7,3},{8,12},{10,14},{12... | collective-permute-start | bytes 786440 | tf_op jit(solution)/shard_map/ppermute | solution.py:377
  51.3 18.4 %all-to-all-start.1 = ((bf16[64,8,128]{2,1,0:T(8,128)(2,1)}), bf16[64,8,128]{2,1,0:T(8,128)(2,1)S(1)}, u32[]{:S(2)}, u32[]{:S(2)}) async-start(bf16[64,8,128]{2,1,0:T(8,128)(2,1)} %bitcast.2), calls=%async_computation.1 | async-start | bytes 262144 | tf_op jit(solution)/shard_map/all_to_all | solution.py:367
  57.9 16.9 %collective-permute-start.2 = (bf16[64,16,128]{2,1,0:T(8,128)(2,1)}, bf16[64,16,128]{2,1,0:T(8,128)(2,1)}, u32[]{:S(2)}, u32[]{:S(2)}) collective-permute-start(bf16[64,16,128]{2,1,0:T(8,128)(2,1)} %slice.45), channel_id=1, source_target_pairs={{0,2},{2,4},{4,6},{6,0},{1,3},{3,5},{5,7},{7,1},{8,10},{10,12},{12... | collective-permute-start | bytes 786440 | tf_op jit(solution)/shard_map/ppermute | solution.py:377
  60.4 15.4 %collective-permute-start.3 = (bf16[64,16,128]{2,1,0:T(8,128)(2,1)}, bf16[64,16,128]{2,1,0:T(8,128)(2,1)S(1)}, u32[]{:S(2)}, u32[]{:S(2)}) collective-permute-start(bf16[64,16,128]{2,1,0:T(8,128)(2,1)} %slice.45), channel_id=1, source_target_pairs={{0,6},{2,0},{4,2},{6,4},{1,7},{3,1},{5,3},{7,5},{8,14},{10,8},{12,... | collective-permute-start | bytes 786440 | tf_op jit(solution)/shard_map/ppermute | solution.py:377
  65.0 37.6 %copy-start.5 = (f32[32,256]{1,0:T(8,128)S(1)}, f32[32,256]{1,0:T(8,128)}, u32[]{:S(2)}) copy-start(f32[32,256]{1,0:T(8,128)} %weight_ref.1) | copy-start | bytes 98308
  65.0 37.6 %copy-start.6 = (bf16[32,256]{1,0:T(8,128)(2,1)S(1)}, bf16[32,256]{1,0:T(8,128)(2,1)}, u32[]{:S(2)}) copy-start(bf16[32,256]{1,0:T(8,128)(2,1)} %get-tuple-element.19.own_ref) | copy-start | bytes 49156
  65.1 26.5 %collective-permute-start = (bf16[2048,128]{1,0:T(8,128)(2,1)S(1)}, bf16[2048,128]{1,0:T(8,128)(2,1)S(1)}, u32[]{:S(2)}, u32[]{:S(2)}) collective-permute-start(bf16[2048,128]{1,0:T(8,128)(2,1)S(1)} %bitcast.31), channel_id=1, source_target_pairs={{0,1},{1,0},{2,3},{3,2},{4,5},{5,4},{6,7},{7,6},{8,9},{9,8},{10,11... | collective-permute-start | bytes 1572872 | tf_op jit(solution)/shard_map/ppermute | solution.py:379
  70.5 8.7 %all-to-all-start.2 = ((f32[8,8,128]{2,1,0:T(8,128)}), f32[8,8,128]{2,1,0:T(8,128)S(1)}, u32[]{:S(2)}, u32[]{:S(2)}) async-start(f32[8,8,128]{2,1,0:T(8,128)} %summed.1), calls=%async_computation.2 | async-start | bytes 65536 | tf_op jit(solution)/shard_map/all_to_all | solution.py:368
  80.0 22.7 %all-to-all-start.3 = ((bf16[64,2,640]{2,1,0:T(2,128)(2,1)}), bf16[64,2,640]{2,1,0:T(2,128)(2,1)S(1)}, u32[]{:S(2)}, u32[]{:S(2)}) async-start(bf16[64,2,640]{2,1,0:T(2,128)(2,1)} %get-tuple-element.18), calls=%async_computation.3 | async-start | bytes 327680 | tf_op jit(solution)/shard_map/all_to_all | solution.py:372

commit v5 on v4

--- a/solution.py
+++ b/solution.py
@@ -100,7 +100,6 @@
     factor = factor_ref[...]
     mine = dot32(factor, pick).astype(BF16)
     own_ref[:, :half] = mine
-    own_ref[:, half:] = dot32(factor, pick_other).astype(BF16)
     out_ref[:, :rows, :] = jnp.broadcast_to(mine[None], (shards, rows, half))
     weight_copy.wait()
     old = weight_ref[...].astype(BF16)
@@ -111,6 +110,7 @@
         )
     out_copy = pltpu.make_async_copy(out_ref, out_hbm, sems.at[0])
     out_copy.start()
+    own_ref[:, half:] = dot32(factor, pick_other).astype(BF16)
     out_copy.wait()
 
 
@@ -196,33 +196,41 @@
 
 
 def moments_step_body(part_ref, moments_ref, message_ref, first_ref, second_ref):
-    lines = first_ref.shape[0]
+    lines = moments_ref.shape[0] // 2
     core = lax.axis_index("tp")
     total = part_ref[:lines, :]
     for i in range(lines, part_ref.shape[0], lines):
         total = total + part_ref[i : i + lines, :]
     new_first = 0.9 * moments_ref[:lines, :] + 0.1 * total
     new_second = 0.95 * moments_ref[lines:, :] + 0.05 * total * total
-    first_ref[...] = new_first
-    second_ref[...] = new_second
     direction = (new_first / (jnp.sqrt(new_second) + 1e-08)).astype(BF16).astype(F32)
     squares = direction * direction
     squares = jnp.sum(jnp.sum(squares, axis=1, keepdims=True), axis=0, keepdims=True)
-    own = []
     tiles = lines // 8
+
+    def own_row(value, pair, parity):
+        base = (parity * 2 + pair) * 2 * tiles
+        return jnp.concatenate(
+            [
+                jnp.where(
+                    core == 0,
+                    value[base + tile : base + tile + 1],
+                    value[base + tiles + tile : base + tiles + tile + 1],
+                )
+                for tile in range(tiles)
+            ],
+            axis=1,
+        )
+
     for pair in range(2):
-        made = []
         for parity in range(2):
-            base = (parity * 2 + pair) * 2 * tiles
-            for tile in range(tiles):
-                made.append(
-                    jnp.where(
-                        core == 0,
-                        direction[base + tile : base + tile + 1],
-                        direction[base + tiles + tile : base + tiles + tile + 1],
-                    )
-                )
-        own.append(jnp.concatenate(made, axis=1))
+            row = pair * 2 + parity
+            first_ref[row : row + 1, :] = own_row(new_first, pair, parity)
+            second_ref[row : row + 1, :] = own_row(new_second, pair, parity)
+    own = [
+        jnp.concatenate([own_row(direction, pair, parity) for parity in range(2)], axis=1)
+        for pair in range(2)
+    ]
     high = squares.astype(BF16).astype(F32)
     middle = (squares - high).astype(BF16).astype(F32)
     low = squares - high - middle
@@ -240,8 +248,8 @@
         moments_step_body,
         out_shape=(
             jax.ShapeDtypeStruct((shards, 2, lines * 32 + 128), BF16),
-            jax.ShapeDtypeStruct((lines, 128), F32),
-            jax.ShapeDtypeStruct((lines, 128), F32),
+            jax.ShapeDtypeStruct((4, lines * 16), F32),
+            jax.ShapeDtypeStruct((4, lines * 16), F32),
         ),
         in_specs=2 * [VMEM_SPEC],
         out_specs=3 * (VMEM_SPEC,),
@@ -342,7 +350,6 @@
     shards = lax.axis_size("fs")
     reps = lax.axis_size("rep")
     rep = lax.axis_index("rep")
-    core = lax.axis_index("tp")
     half = factor.shape[1] // 2
     rows, cols = weight.shape
     tiles = cols // 128
@@ -382,17 +389,12 @@
         gathered, sent, factor_other, old_all, own_factor, weight
     )
 
-    def own_entries(value):
-        value = value.reshape(2, pairs, 2, tiles * 128)
-        value = jnp.where(core == 0, value[:, :, 0], value[:, :, 1])
-        return jnp.stack([value[0], value[1]], axis=1).reshape(own_rows, cols)
-
     return (
         new_weight,
         copies.reshape(-1, cols),
         update_step,
-        own_entries(new_first),
-        own_entries(new_second),
+        new_first,
+        new_second,
     )
 
 

time: 105 us -> 105 us (level)
  waiting for transfers between devices: 28.1 us -> 29.4 us
  local copies, waits for them, and re-layouts: 8.99 us -> 7.74 us
    reshape x4 -> x0, local copies, waits for them, and re-layouts: 1.24 us -> none  [the longest x2 1.22 us: own_entries(): return jnp.stack([value[0], value[1]], axis=1).reshape(own_rows, cols)]
    all_to_all x1, waiting for transfers between devices: 3.28 us -> 4.35 us  [on_device(): lax.all_to_all(summed(arrived, 2 * reps), ('rep', 'tp'), 0, 0, tiled=True)]
  transfers between devices with their start and end apart: 8 -> 8, of which waited for: 4 -> 4; matrix products, arithmetic and copies ran while one was open for 4% -> 3% of each run, Pallas kernels for 7% -> 7%
where the time goes in v5:
time: 105 us; the launch traced here: 104 us
  starting transfers between devices  50.7 us (48%)
  waiting for transfers between devices  29.4 us (28%)
  Pallas kernels  10.9 us (10%)
  local copies, waits for them, and re-layouts  7.74 us (7%)
  blocking collectives  3.99 us (4%)
    all_to_all x1, starting transfers between devices, on_device(): sent = lax.all_to_all(message, 'fs', 0, 0, tiled=True)  16.7 us
    ppermute x3, starting transfers between devices, on_device(): lax.ppermute(old_mine, 'rep', [(j, (j + i) % reps) for j in range(reps)])  12 us
    all_to_all x1, waiting for transfers between devices, on_device(): gathered = lax.all_to_all(message, 'fs', 0, 0, tiled=True)  11.3 us
    all_to_all x1, waiting for transfers between devices, on_device(): sent = lax.all_to_all(message, 'fs', 0, 0, tiled=True)  11.2 us
    all_to_all x1, starting transfers between devices, on_device(): gathered = lax.all_to_all(message, 'fs', 0, 0, tiled=True)  10.2 us
    all_to_all x1, starting transfers between devices, on_device(): lax.all_to_all(sums.reshape(shards, lines // 2, 128), 'fs', 0, 0, tiled=T...  6.52 us
    unnamed x16, local copies, waits for them, and re-layouts  4.65 us
    all_to_all x1, waiting for transfers between devices, on_device(): lax.all_to_all(summed(arrived, 2 * reps), ('rep', 'tp'), 0, 0, tiled=True)  4.35 us
  transfers between devices with their start and end apart: 8, of which 4 were waited for; matrix products, arithmetic and copies ran while one was open for 3% of the time, Pallas kernels for 7%

profile of v5, /device:TPU:8, one launch (start us, length us, event | category | flops | bytes accessed | tf_op | source)
XLA Modules:
  0.0 104.3 jit_solution(14050926288349803639)
XLA Ops:
  0.6 2.4 %first_message.1 = (bf16[64,48,128]{2,1,0:T(8,128)(2,1)}, bf16[32,256]{1,0:T(8,128)(2,1)}) custom-call(bf16[32,256]{1,0:T(8,128)(2,1)} %factor_hbm.1, f32[32,256]{1,0:T(8,128)} %weight_ref.1), custom_call_target="tpu_custom_call" | custom-call | tf_op jit(solution)/shard_map/first_message/pallas_call | solution.py:123
  3.1 0.0 copy-start
  3.1 16.7 %all-to-all-start = ((bf16[64,48,128]{2,1,0:T(8,128)(2,1)}), bf16[64,48,128]{2,1,0:T(8,128)(2,1)S(1)}, u32[]{:S(2)}, u32[]{:S(2)}) async-start(bf16[64,48,128]{2,1,0:T(8,128)(2,1)} %get-tuple-element.15), calls=%async_computation | async-start | bytes 1572864 | tf_op jit(solution)/shard_map/all_to_all | solution.py:361
  19.8 0.7 pad_maximum_fusion
  20.5 1.8 %all-gather = f32[16,256]{1,0:T(8,128)S(1)} all-gather(f32[8,256]{1,0:T(8,128)S(1)} %pad_maximum_fusion), channel_id=2, replica_groups=mesh['fs'=64,'rep'=4,'tp'=2] {'tp'}, dimensions={0}, use_global_device_ids=true | all-gather | bytes 24576 | tf_op jit(solution)/shard_map/all_gather | solution.py:365
  22.3 0.0 copy-start.1
  22.4 1.0 copy-done.1
  23.4 0.0 copy-start.2
  23.4 1.0 copy-done.2
  24.4 0.0 copy-start.3
  24.4 0.9 copy-done.3
  25.4 0.0 copy-start.4
  25.4 0.9 copy-done.4
  26.3 0.0 copy-start.7
  26.3 0.7 copy-done.7
  27.0 3.4 %key_gradient.1 = bf16[512,256]{1,0:T(8,128)(2,1)S(1)} custom-call(f32[4]{0:T(128)S(1)} %copy-done.7, bf16[512,256]{1,0:T(8,128)(2,1)S(1)} %copy-done.3, bf16[512,256]{1,0:T(8,128)(2,1)S(1)} %copy-done.4, bf16[512,512]{1,0:T(8,128)(2,1)S(1)} %copy-done.1, bf16[512,512]{1,0:T(8,128)(2,1)S(1)} %copy-done.2), custom_call_target="tpu_custom_call" | custom-call | tf_op jit(solution)/shard_map/key_gradient/pallas_call | solution.py:70
  30.4 2.2 %all_gather.11.grad_ref = bf16[1024,256]{1,0:T(8,128)(2,1)S(1)} all-gather(bf16[512,256]{1,0:T(8,128)(2,1)S(1)} %key_gradient.1), channel_id=1, replica_groups=mesh['fs'=64,'rep'=4,'tp'=2] {'tp'}, dimensions={0}, use_global_device_ids=true | all-gather | bytes 786432 | tf_op jit(solution)/shard_map/all_gather | solution.py:370
  32.6 11.2 %all-to-all-done.sent_ref = bf16[64,48,128]{2,1,0:T(8,128)(2,1)S(1)} async-done(((bf16[64,48,128]{2,1,0:T(8,128)(2,1)}), bf16[64,48,128]{2,1,0:T(8,128)(2,1)S(1)}, u32[]{:S(2)}, u32[]{:S(2)}) %all-to-all-start) | async-done | bytes 786464 | tf_op jit(solution)/shard_map/all_to_all | solution.py:361
  43.8 0.7 slice.9
  44.5 4.9 %collective-permute-start.1 = (bf16[64,16,128]{2,1,0:T(8,128)(2,1)}, bf16[64,16,128]{2,1,0:T(8,128)(2,1)}, u32[]{:S(2)}, u32[]{:S(2)}) collective-permute-start(bf16[64,16,128]{2,1,0:T(8,128)(2,1)} %slice.9), channel_id=1, source_target_pairs={{0,4},{2,6},{4,0},{6,2},{1,5},{3,7},{5,1},{7,3},{8,12},{10,14},{12... | collective-permute-start | bytes 786440 | tf_op jit(solution)/shard_map/ppermute | solution.py:384
  49.4 0.0 copy-done
  49.4 1.9 %projected_sums.1 = bf16[512,128]{1,0:T(8,128)(2,1)} custom-call(bf16[512,2048]{1,0:T(8,128)(2,1)S(1)} %copy-done, bf16[64,48,128]{2,1,0:T(8,128)(2,1)S(1)} %all-to-all-done.sent_ref, bf16[1024,256]{1,0:T(8,128)(2,1)S(1)} %all_gather.11.grad_ref), custom_call_target="tpu_custom_call" | custom-call | flops 536870912 | bytes 2097152 | tf_op jit(solution)/shard_map/projected_sums/pallas_call | solution.py:168
  51.3 6.5 %all-to-all-start.1 = ((bf16[64,8,128]{2,1,0:T(8,128)(2,1)}), bf16[64,8,128]{2,1,0:T(8,128)(2,1)S(1)}, u32[]{:S(2)}, u32[]{:S(2)}) async-start(bf16[64,8,128]{2,1,0:T(8,128)(2,1)} %bitcast.2), calls=%async_computation.1 | async-start | bytes 262144 | tf_op jit(solution)/shard_map/all_to_all | solution.py:374
  57.9 2.5 %collective-permute-start.2 = (bf16[64,16,128]{2,1,0:T(8,128)(2,1)}, bf16[64,16,128]{2,1,0:T(8,128)(2,1)}, u32[]{:S(2)}, u32[]{:S(2)}) collective-permute-start(bf16[64,16,128]{2,1,0:T(8,128)(2,1)} %slice.9), channel_id=1, source_target_pairs={{0,2},{2,4},{4,6},{6,0},{1,3},{3,5},{5,7},{7,1},{8,10},{10,12},{12... | collective-permute-start | bytes 786440 | tf_op jit(solution)/shard_map/ppermute | solution.py:384
  60.4 4.6 %collective-permute-start.3 = (bf16[64,16,128]{2,1,0:T(8,128)(2,1)}, bf16[64,16,128]{2,1,0:T(8,128)(2,1)S(1)}, u32[]{:S(2)}, u32[]{:S(2)}) collective-permute-start(bf16[64,16,128]{2,1,0:T(8,128)(2,1)} %slice.9), channel_id=1, source_target_pairs={{0,6},{2,0},{4,2},{6,4},{1,7},{3,1},{5,3},{7,5},{8,14},{10,8},{12,... | collective-permute-start | bytes 786440 | tf_op jit(solution)/shard_map/ppermute | solution.py:384
  65.0 0.0 copy-start.5
  65.0 0.0 copy-start.6
  65.1 1.9 %collective-permute-start = (bf16[2048,128]{1,0:T(8,128)(2,1)S(1)}, bf16[2048,128]{1,0:T(8,128)(2,1)S(1)}, u32[]{:S(2)}, u32[]{:S(2)}) collective-permute-start(bf16[2048,128]{1,0:T(8,128)(2,1)S(1)} %bitcast.23), channel_id=1, source_target_pairs={{0,1},{1,0},{2,3},{3,2},{4,5},{5,4},{6,7},{7,6},{8,9},{9,8},{10,11... | collective-permute-start | bytes 1572872 | tf_op jit(solution)/shard_map/ppermute | solution.py:386
  67.0 0.2 broadcast_in_dim.16
  67.3 2.5 %all-to-all-done.1.arrived_ref = bf16[64,8,128]{2,1,0:T(8,128)(2,1)S(1)} async-done(((bf16[64,8,128]{2,1,0:T(8,128)(2,1)}), bf16[64,8,128]{2,1,0:T(8,128)(2,1)S(1)}, u32[]{:S(2)}, u32[]{:S(2)}) %all-to-all-start.1) | async-done | bytes 131104 | tf_op jit(solution)/shard_map/all_to_all | solution.py:374
  69.8 0.7 summed.1
  70.5 3.3 %all-to-all-start.2 = ((f32[8,8,128]{2,1,0:T(8,128)}), f32[8,8,128]{2,1,0:T(8,128)S(1)}, u32[]{:S(2)}, u32[]{:S(2)}) async-start(f32[8,8,128]{2,1,0:T(8,128)} %summed.1), calls=%async_computation.2 | async-start | bytes 65536 | tf_op jit(solution)/shard_map/all_to_all | solution.py:375
  73.8 0.0 collective-permute-done.1
  73.8 1.0 bitcast_dynamic-update-slice_fusion.1
  74.8 4.4 %all-to-all-done.2 = f32[8,8,128]{2,1,0:T(8,128)S(1)} async-done(((f32[8,8,128]{2,1,0:T(8,128)}), f32[8,8,128]{2,1,0:T(8,128)S(1)}, u32[]{:S(2)}, u32[]{:S(2)}) %all-to-all-start.2) | async-done | bytes 32800 | tf_op jit(solution)/shard_map/all_to_all | solution.py:375
  79.2 0.8 moments_step.1
  80.0 10.2 %all-to-all-start.3 = ((bf16[64,2,640]{2,1,0:T(2,128)(2,1)}), bf16[64,2,640]{2,1,0:T(2,128)(2,1)S(1)}, u32[]{:S(2)}, u32[]{:S(2)}) async-start(bf16[64,2,640]{2,1,0:T(2,128)(2,1)} %get-tuple-element.18), calls=%async_computation.3 | async-start | bytes 327680 | tf_op jit(solution)/shard_map/all_to_all | solution.py:379
  90.2 0.0 collective-permute-done.2
  90.2 1.0 bitcast_dynamic-update-slice_fusion
  91.2 0.0 collective-permute-done.3
  91.3 0.0 collective-permute-done.swapped_ref
  91.3 11.3 %all-to-all-done.3.gathered_ref = bf16[64,2,640]{2,1,0:T(2,128)(2,1)S(1)} async-done(((bf16[64,2,640]{2,1,0:T(2,128)(2,1)}), bf16[64,2,640]{2,1,0:T(2,128)(2,1)S(1)}, u32[]{:S(2)}, u32[]{:S(2)}) %all-to-all-start.3) | async-done | bytes 163872 | tf_op jit(solution)/shard_map/all_to_all | solution.py:379
  102.6 0.0 copy-done.5
  102.6 0.0 copy-done.6
  102.6 1.7 %new_weights.1 = (bf16[64,4,8,256]{3,2,1,0:T(8,128)(2,1)}, f32[32,256]{1,0:T(8,128)}, f32[32,256]{1,0:T(8,128)}) custom-call(bf16[64,2,640]{2,1,0:T(2,128)(2,1)S(1)} %all-to-all-done.3.gathered_ref, bf16[64,48,128]{2,1,0:T(8,128)(2,1)S(1)} %all-to-all-done.sent_ref, bf16[2048,128]{1,0:T(8,128)(2,1)S(1)} %collective-permute-done.swapped_ref, ...), custom_call_target="tpu_custom_call" | custom-call | flops 268435456 | bytes 2097152 | tf_op jit(solution)/shard_map/new_weights/pallas_call | solution.py:321
  (5 shorter events, 0.1 us)
Async XLA Ops:
  3.1 46.4 %copy-start = (bf16[512,2048]{1,0:T(8,128)(2,1)S(1)}, bf16[512,2048]{1,0:T(8,128)(2,1)}, u32[]{:S(2)}) copy-start(bf16[512,2048]{1,0:T(8,128)(2,1)} %tokens_ref.1) | copy-start | bytes 6291460
  3.1 40.7 %all-to-all-start = ((bf16[64,48,128]{2,1,0:T(8,128)(2,1)}), bf16[64,48,128]{2,1,0:T(8,128)(2,1)S(1)}, u32[]{:S(2)}, u32[]{:S(2)}) async-start(bf16[64,48,128]{2,1,0:T(8,128)(2,1)} %get-tuple-element.15), calls=%async_computation | async-start | bytes 1572864 | tf_op jit(solution)/shard_map/all_to_all | solution.py:361
  22.3 1.0 %copy-start.1 = (bf16[512,512]{1,0:T(8,128)(2,1)S(1)}, bf16[512,512]{1,0:T(8,128)(2,1)}, u32[]{:S(2)}) copy-start(bf16[512,512]{1,0:T(8,128)(2,1)} %value_ref.1) | copy-start | bytes 1572868
  23.4 1.0 copy-start.2
  24.4 0.9 copy-start.3
  25.4 0.9 copy-start.4
  26.3 0.7 copy-start.7
  44.5 29.3 %collective-permute-start.1 = (bf16[64,16,128]{2,1,0:T(8,128)(2,1)}, bf16[64,16,128]{2,1,0:T(8,128)(2,1)}, u32[]{:S(2)}, u32[]{:S(2)}) collective-permute-start(bf16[64,16,128]{2,1,0:T(8,128)(2,1)} %slice.9), channel_id=1, source_target_pairs={{0,4},{2,6},{4,0},{6,2},{1,5},{3,7},{5,1},{7,3},{8,12},{10,14},{12... | collective-permute-start | bytes 786440 | tf_op jit(solution)/shard_map/ppermute | solution.py:384
  51.3 18.4 %all-to-all-start.1 = ((bf16[64,8,128]{2,1,0:T(8,128)(2,1)}), bf16[64,8,128]{2,1,0:T(8,128)(2,1)S(1)}, u32[]{:S(2)}, u32[]{:S(2)}) async-start(bf16[64,8,128]{2,1,0:T(8,128)(2,1)} %bitcast.2), calls=%async_computation.1 | async-start | bytes 262144 | tf_op jit(solution)/shard_map/all_to_all | solution.py:374
  57.9 32.3 %collective-permute-start.2 = (bf16[64,16,128]{2,1,0:T(8,128)(2,1)}, bf16[64,16,128]{2,1,0:T(8,128)(2,1)}, u32[]{:S(2)}, u32[]{:S(2)}) collective-permute-start(bf16[64,16,128]{2,1,0:T(8,128)(2,1)} %slice.9), channel_id=1, source_target_pairs={{0,2},{2,4},{4,6},{6,0},{1,3},{3,5},{5,7},{7,1},{8,10},{10,12},{12... | collective-permute-start | bytes 786440 | tf_op jit(solution)/shard_map/ppermute | solution.py:384
  60.4 30.8 %collective-permute-start.3 = (bf16[64,16,128]{2,1,0:T(8,128)(2,1)}, bf16[64,16,128]{2,1,0:T(8,128)(2,1)S(1)}, u32[]{:S(2)}, u32[]{:S(2)}) collective-permute-start(bf16[64,16,128]{2,1,0:T(8,128)(2,1)} %slice.9), channel_id=1, source_target_pairs={{0,6},{2,0},{4,2},{6,4},{1,7},{3,1},{5,3},{7,5},{8,14},{10,8},{12,... | collective-permute-start | bytes 786440 | tf_op jit(solution)/shard_map/ppermute | solution.py:384
  65.0 37.6 %copy-start.5 = (f32[32,256]{1,0:T(8,128)S(1)}, f32[32,256]{1,0:T(8,128)}, u32[]{:S(2)}) copy-start(f32[32,256]{1,0:T(8,128)} %weight_ref.1) | copy-start | bytes 98308
  65.0 37.6 %copy-start.6 = (bf16[32,256]{1,0:T(8,128)(2,1)S(1)}, bf16[32,256]{1,0:T(8,128)(2,1)}, u32[]{:S(2)}) copy-start(bf16[32,256]{1,0:T(8,128)(2,1)} %get-tuple-element.19.own_ref) | copy-start | bytes 49156
  65.1 26.2 %collective-permute-start = (bf16[2048,128]{1,0:T(8,128)(2,1)S(1)}, bf16[2048,128]{1,0:T(8,128)(2,1)S(1)}, u32[]{:S(2)}, u32[]{:S(2)}) collective-permute-start(bf16[2048,128]{1,0:T(8,128)(2,1)S(1)} %bitcast.23), channel_id=1, source_target_pairs={{0,1},{1,0},{2,3},{3,2},{4,5},{5,4},{6,7},{7,6},{8,9},{9,8},{10,11... | collective-permute-start | bytes 1572872 | tf_op jit(solution)/shard_map/ppermute | solution.py:386
  70.5 8.7 %all-to-all-start.2 = ((f32[8,8,128]{2,1,0:T(8,128)}), f32[8,8,128]{2,1,0:T(8,128)S(1)}, u32[]{:S(2)}, u32[]{:S(2)}) async-start(f32[8,8,128]{2,1,0:T(8,128)} %summed.1), calls=%async_computation.2 | async-start | bytes 65536 | tf_op jit(solution)/shard_map/all_to_all | solution.py:375
  80.0 22.7 %all-to-all-start.3 = ((bf16[64,2,640]{2,1,0:T(2,128)(2,1)}), bf16[64,2,640]{2,1,0:T(2,128)(2,1)S(1)}, u32[]{:S(2)}, u32[]{:S(2)}) async-start(bf16[64,2,640]{2,1,0:T(2,128)(2,1)} %get-tuple-element.18), calls=%async_computation.3 | async-start | bytes 327680 | tf_op jit(solution)/shard_map/all_to_all | solution.py:379

commit v6 on v5

--- a/solution.py
+++ b/solution.py
@@ -139,10 +139,12 @@
     )(factor, weight)
 
 
-def projected_sums_body(tokens_ref, sent_ref, grad_ref, out_ref, laid_ref):
+def projected_sums_body(tokens_ref, sent_ref, grad_ref, out_ref, old_hbm, laid_ref, sem):
     shards, _, half = sent_ref.shape
     length, width = tokens_ref.shape
     rows = width // shards
+    old_copy = pltpu.make_async_copy(sent_ref.at[:, rows:, :], old_hbm, sem)
+    old_copy.start()
     cols = grad_ref.shape[1]
     pairs = half // shards
     factor = sent_ref[:, :rows, :].reshape(width, half)
@@ -160,17 +162,19 @@
                     pair * shards : pair * shards + shards, tile * 128 : tile * 128 + 128
                 ]
     out_ref[...] = laid_ref[...].astype(BF16)
+    old_copy.wait()
 
 
 def projected_sums(tokens, sent, grads):
-    half = sent.shape[2]
+    shards, sent_rows, half = sent.shape
     total = half * 2 * grads.shape[1] // 128
+    old = (shards, sent_rows - tokens.shape[1] // shards, half)
     return pl.pallas_call(
         projected_sums_body,
-        out_shape=jax.ShapeDtypeStruct((total, 128), BF16),
+        out_shape=(jax.ShapeDtypeStruct((total, 128), BF16), pltpu.HBM(old, BF16)),
         in_specs=3 * [VMEM_SPEC],
-        out_specs=VMEM_SPEC,
-        scratch_shapes=[pltpu.VMEM((total, 128), F32)],
+        out_specs=(VMEM_SPEC, pl.BlockSpec(memory_space=pltpu.HBM)),
+        scratch_shapes=[pltpu.VMEM((total, 128), F32), pltpu.SemaphoreType.DMA],
         cost_estimate=pl.CostEstimate(
             flops=4 * tokens.size * half, bytes_accessed=2 * tokens.size, transcendentals=0
         ),
@@ -359,7 +363,6 @@
 
     message, own_factor = first_message(factor, weight, shards, reps)
     sent = lax.all_to_all(message, "fs", 0, 0, tiled=True)
-    old_mine = sent[:, rows:]
     factor_mine = sent[:, :rows].reshape(-1, half)
 
     moments = lax.all_gather(jnp.concatenate([first_moment, second_moment], 0), "tp")
@@ -370,7 +373,7 @@
     key_both = lax.all_gather(key_grad, "tp", tiled=True)
     moments, key_both = lax.optimization_barrier((moments, key_both))
 
-    sums = projected_sums(tokens_in, sent, key_both)
+    sums, old_mine = projected_sums(tokens_in, sent, key_both)
     arrived = lax.all_to_all(sums.reshape(shards, lines // 2, 128), "fs", 0, 0, tiled=True)
     part = lax.all_to_all(summed(arrived, 2 * reps), ("rep", "tp"), 0, 0, tiled=True)
     message, new_first, new_second = moments_step(

time: 105 us -> 105 us (level)
    unnamed x16 -> x18, local copies, waits for them, and re-layouts: 4.65 us -> 4.66 us
  transfers between devices with their start and end apart: 8 -> 8, of which waited for: 4 -> 4; matrix products, arithmetic and copies ran while one was open for 3% -> 4% of each run, Pallas kernels for 7% -> 5%
where the time goes in v6:
time: 105 us; the launch traced here: 104 us
  starting transfers between devices  50.9 us (48%)
  waiting for transfers between devices  28.4 us (27%)
  Pallas kernels  11 us (10%)
  local copies, waits for them, and re-layouts  7.98 us (8%)
  blocking collectives  3.99 us (4%)
    all_to_all x1, starting transfers between devices, on_device(): sent = lax.all_to_all(message, 'fs', 0, 0, tiled=True)  16.7 us
    ppermute x3, starting transfers between devices, on_device(): lax.ppermute(old_mine, 'rep', [(j, (j + i) % reps) for j in range(reps)])  12.1 us
    all_to_all x1, waiting for transfers between devices, on_device(): sent = lax.all_to_all(message, 'fs', 0, 0, tiled=True)  11.2 us
    all_to_all x1, waiting for transfers between devices, on_device(): gathered = lax.all_to_all(message, 'fs', 0, 0, tiled=True)  10.4 us
    all_to_all x1, starting transfers between devices, on_device(): gathered = lax.all_to_all(message, 'fs', 0, 0, tiled=True)  10.2 us
    all_to_all x1, starting transfers between devices, on_device(): lax.all_to_all(sums.reshape(shards, lines // 2, 128), 'fs', 0, 0, tiled=T...  6.53 us
    unnamed x18, local copies, waits for them, and re-layouts  4.66 us
    all_to_all x1, waiting for transfers between devices, on_device(): lax.all_to_all(summed(arrived, 2 * reps), ('rep', 'tp'), 0, 0, tiled=True)  4.35 us
  transfers between devices with their start and end apart: 8, of which 4 were waited for; matrix products, arithmetic and copies ran while one was open for 4% of the time, Pallas kernels for 5%

profile of v6, /device:TPU:8, one launch (start us, length us, event | category | flops | bytes accessed | tf_op | source)
XLA Modules:
  0.0 103.8 jit_solution(5602467447994535761)
XLA Ops:
  0.6 2.4 %first_message.1 = (bf16[64,48,128]{2,1,0:T(8,128)(2,1)}, bf16[32,256]{1,0:T(8,128)(2,1)}) custom-call(bf16[32,256]{1,0:T(8,128)(2,1)} %factor_hbm.1, f32[32,256]{1,0:T(8,128)} %weight_ref.1), custom_call_target="tpu_custom_call" | custom-call | tf_op jit(solution)/shard_map/first_message/pallas_call | solution.py:123
  3.1 0.0 copy-start
  3.1 16.7 %all-to-all-start = ((bf16[64,48,128]{2,1,0:T(8,128)(2,1)}), bf16[64,48,128]{2,1,0:T(8,128)(2,1)S(1)}, u32[]{:S(2)}, u32[]{:S(2)}) async-start(bf16[64,48,128]{2,1,0:T(8,128)(2,1)} %get-tuple-element.17), calls=%async_computation | async-start | bytes 1572864 | tf_op jit(solution)/shard_map/all_to_all | solution.py:365
  19.8 0.7 pad_maximum_fusion
  20.5 1.8 %all-gather = f32[16,256]{1,0:T(8,128)S(1)} all-gather(f32[8,256]{1,0:T(8,128)S(1)} %pad_maximum_fusion), channel_id=2, replica_groups=mesh['fs'=64,'rep'=4,'tp'=2] {'tp'}, dimensions={0}, use_global_device_ids=true | all-gather | bytes 24576 | tf_op jit(solution)/shard_map/all_gather | solution.py:368
  22.3 0.0 copy-start.1
  22.4 1.0 copy-done.1
  23.4 0.0 copy-start.2
  23.4 1.0 %copy-done.2 = bf16[512,512]{1,0:T(8,128)(2,1)S(1)} copy-done((bf16[512,512]{1,0:T(8,128)(2,1)S(1)}, bf16[512,512]{1,0:T(8,128)(2,1)}, u32[]{:S(2)}) %copy-start.2) | copy-done | bytes 524312
  24.4 0.0 copy-start.3
  24.4 0.9 copy-done.3
  25.4 0.0 copy-start.4
  25.4 0.9 copy-done.4
  26.3 0.0 copy-start.7
  26.3 0.7 copy-done.7
  27.0 3.4 %key_gradient.1 = bf16[512,256]{1,0:T(8,128)(2,1)S(1)} custom-call(f32[4]{0:T(128)S(1)} %copy-done.7, bf16[512,256]{1,0:T(8,128)(2,1)S(1)} %copy-done.3, bf16[512,256]{1,0:T(8,128)(2,1)S(1)} %copy-done.4, bf16[512,512]{1,0:T(8,128)(2,1)S(1)} %copy-done.1, bf16[512,512]{1,0:T(8,128)(2,1)S(1)} %copy-done.2), custom_call_target="tpu_custom_call" | custom-call | tf_op jit(solution)/shard_map/key_gradient/pallas_call | solution.py:70
  30.4 2.2 %all_gather.11.grad_ref = bf16[1024,256]{1,0:T(8,128)(2,1)S(1)} all-gather(bf16[512,256]{1,0:T(8,128)(2,1)S(1)} %key_gradient.1), channel_id=1, replica_groups=mesh['fs'=64,'rep'=4,'tp'=2] {'tp'}, dimensions={0}, use_global_device_ids=true | all-gather | bytes 786432 | tf_op jit(solution)/shard_map/all_gather | solution.py:373
  32.6 11.2 %all-to-all-done.sent_ref = bf16[64,48,128]{2,1,0:T(8,128)(2,1)S(1)} async-done(((bf16[64,48,128]{2,1,0:T(8,128)(2,1)}), bf16[64,48,128]{2,1,0:T(8,128)(2,1)S(1)}, u32[]{:S(2)}, u32[]{:S(2)}) %all-to-all-start) | async-done | bytes 786464 | tf_op jit(solution)/shard_map/all_to_all | solution.py:365
  43.8 0.0 copy-done
  43.8 1.9 %projected_sums.1 = (bf16[512,128]{1,0:T(8,128)(2,1)}, bf16[64,16,128]{2,1,0:T(8,128)(2,1)}) custom-call(bf16[512,2048]{1,0:T(8,128)(2,1)S(1)} %copy-done, bf16[64,48,128]{2,1,0:T(8,128)(2,1)S(1)} %all-to-all-done.sent_ref, bf16[1024,256]{1,0:T(8,128)(2,1)S(1)} %all_gather.11.grad_ref), custom_call_target="tpu_custom_call" | custom-call | flops 536870912 | bytes 2097152 | tf_op jit(solution)/shard_map/projected_sums/pallas_call | solution.py:172
  45.7 0.0 copy-start.8
  45.7 5.1 %collective-permute-start.1 = (bf16[64,16,128]{2,1,0:T(8,128)(2,1)}, bf16[64,16,128]{2,1,0:T(8,128)(2,1)}, u32[]{:S(2)}, u32[]{:S(2)}) collective-permute-start(bf16[64,16,128]{2,1,0:T(8,128)(2,1)} %get-tuple-element.22), channel_id=1, source_target_pairs={{0,4},{2,6},{4,0},{6,2},{1,5},{3,7},{5,1},{7,3},{8,12},{10,14},{12... | collective-permute-start | bytes 786440 | tf_op jit(solution)/shard_map/ppermute | solution.py:387
  50.8 6.5 %all-to-all-start.1 = ((bf16[64,8,128]{2,1,0:T(8,128)(2,1)}), bf16[64,8,128]{2,1,0:T(8,128)(2,1)S(1)}, u32[]{:S(2)}, u32[]{:S(2)}) async-start(bf16[64,8,128]{2,1,0:T(8,128)(2,1)} %bitcast.2), calls=%async_computation.1 | async-start | bytes 262144 | tf_op jit(solution)/shard_map/all_to_all | solution.py:377
  57.4 2.5 %collective-permute-start.2 = (bf16[64,16,128]{2,1,0:T(8,128)(2,1)}, bf16[64,16,128]{2,1,0:T(8,128)(2,1)}, u32[]{:S(2)}, u32[]{:S(2)}) collective-permute-start(bf16[64,16,128]{2,1,0:T(8,128)(2,1)} %get-tuple-element.22), channel_id=1, source_target_pairs={{0,2},{2,4},{4,6},{6,0},{1,3},{3,5},{5,7},{7,1},{8,10},{10,12},{12... | collective-permute-start | bytes 786440 | tf_op jit(solution)/shard_map/ppermute | solution.py:387
  59.9 4.6 %collective-permute-start.3 = (bf16[64,16,128]{2,1,0:T(8,128)(2,1)}, bf16[64,16,128]{2,1,0:T(8,128)(2,1)}, u32[]{:S(2)}, u32[]{:S(2)}) collective-permute-start(bf16[64,16,128]{2,1,0:T(8,128)(2,1)} %get-tuple-element.22), channel_id=1, source_target_pairs={{0,6},{2,0},{4,2},{6,4},{1,7},{3,1},{5,3},{7,5},{8,14},{10,8},{12,... | collective-permute-start | bytes 786440 | tf_op jit(solution)/shard_map/ppermute | solution.py:387
  64.5 0.0 copy-start.5
  64.5 0.0 copy-start.6
  64.5 1.9 %collective-permute-start = (bf16[2048,128]{1,0:T(8,128)(2,1)S(1)}, bf16[2048,128]{1,0:T(8,128)(2,1)S(1)}, u32[]{:S(2)}, u32[]{:S(2)}) collective-permute-start(bf16[2048,128]{1,0:T(8,128)(2,1)S(1)} %bitcast.17), channel_id=1, source_target_pairs={{0,1},{1,0},{2,3},{3,2},{4,5},{5,4},{6,7},{7,6},{8,9},{9,8},{10,11... | collective-permute-start | bytes 1572872 | tf_op jit(solution)/shard_map/ppermute | solution.py:389
  66.4 0.2 broadcast_in_dim.16
  66.7 0.0 copy-done.8
  66.8 2.5 %all-to-all-done.1.arrived_ref = bf16[64,8,128]{2,1,0:T(8,128)(2,1)S(1)} async-done(((bf16[64,8,128]{2,1,0:T(8,128)(2,1)}), bf16[64,8,128]{2,1,0:T(8,128)(2,1)S(1)}, u32[]{:S(2)}, u32[]{:S(2)}) %all-to-all-start.1) | async-done | bytes 131104 | tf_op jit(solution)/shard_map/all_to_all | solution.py:377
  69.2 0.7 summed.1
  69.9 3.3 %all-to-all-start.2 = ((f32[8,8,128]{2,1,0:T(8,128)}), f32[8,8,128]{2,1,0:T(8,128)S(1)}, u32[]{:S(2)}, u32[]{:S(2)}) async-start(f32[8,8,128]{2,1,0:T(8,128)} %summed.1), calls=%async_computation.2 | async-start | bytes 65536 | tf_op jit(solution)/shard_map/all_to_all | solution.py:378
  73.3 0.0 collective-permute-done.1
  73.3 1.0 bitcast_dynamic-update-slice_fusion.2
  74.3 4.4 %all-to-all-done.2 = f32[8,8,128]{2,1,0:T(8,128)S(1)} async-done(((f32[8,8,128]{2,1,0:T(8,128)}), f32[8,8,128]{2,1,0:T(8,128)S(1)}, u32[]{:S(2)}, u32[]{:S(2)}) %all-to-all-start.2) | async-done | bytes 32800 | tf_op jit(solution)/shard_map/all_to_all | solution.py:378
  78.6 0.8 moments_step.1
  79.5 10.2 %all-to-all-start.3 = ((bf16[64,2,640]{2,1,0:T(2,128)(2,1)}), bf16[64,2,640]{2,1,0:T(2,128)(2,1)S(1)}, u32[]{:S(2)}, u32[]{:S(2)}) async-start(bf16[64,2,640]{2,1,0:T(2,128)(2,1)} %get-tuple-element.21), calls=%async_computation.3 | async-start | bytes 327680 | tf_op jit(solution)/shard_map/all_to_all | solution.py:382
  89.7 0.0 collective-permute-done.2
  89.7 1.0 bitcast_dynamic-update-slice_fusion.1
  90.7 0.0 collective-permute-done.3
  90.7 1.0 bitcast_dynamic-update-slice_fusion.old_ref
  91.7 0.0 collective-permute-done.swapped_ref
  91.7 10.4 %all-to-all-done.3.gathered_ref = bf16[64,2,640]{2,1,0:T(2,128)(2,1)S(1)} async-done(((bf16[64,2,640]{2,1,0:T(2,128)(2,1)}), bf16[64,2,640]{2,1,0:T(2,128)(2,1)S(1)}, u32[]{:S(2)}, u32[]{:S(2)}) %all-to-all-start.3) | async-done | bytes 163872 | tf_op jit(solution)/shard_map/all_to_all | solution.py:382
  102.1 0.0 copy-done.5
  102.1 0.0 copy-done.6
  102.1 1.7 %new_weights.1 = (bf16[64,4,8,256]{3,2,1,0:T(8,128)(2,1)}, f32[32,256]{1,0:T(8,128)}, f32[32,256]{1,0:T(8,128)}) custom-call(bf16[64,2,640]{2,1,0:T(2,128)(2,1)S(1)} %all-to-all-done.3.gathered_ref, bf16[64,48,128]{2,1,0:T(8,128)(2,1)S(1)} %all-to-all-done.sent_ref, bf16[2048,128]{1,0:T(8,128)(2,1)S(1)} %collective-permute-done.swapped_ref, ...), custom_call_target="tpu_custom_call" | custom-call | flops 268435456 | bytes 2097152 | tf_op jit(solution)/shard_map/new_weights/pallas_call | solution.py:325
  (4 shorter events, 0.1 us)
Async XLA Ops:
  3.1 40.7 %copy-start = (bf16[512,2048]{1,0:T(8,128)(2,1)S(1)}, bf16[512,2048]{1,0:T(8,128)(2,1)}, u32[]{:S(2)}) copy-start(bf16[512,2048]{1,0:T(8,128)(2,1)} %tokens_ref.1) | copy-start | bytes 6291460
  3.1 40.7 %all-to-all-start = ((bf16[64,48,128]{2,1,0:T(8,128)(2,1)}), bf16[64,48,128]{2,1,0:T(8,128)(2,1)S(1)}, u32[]{:S(2)}, u32[]{:S(2)}) async-start(bf16[64,48,128]{2,1,0:T(8,128)(2,1)} %get-tuple-element.17), calls=%async_computation | async-start | bytes 1572864 | tf_op jit(solution)/shard_map/all_to_all | solution.py:365
  22.3 1.0 %copy-start.1 = (bf16[512,512]{1,0:T(8,128)(2,1)S(1)}, bf16[512,512]{1,0:T(8,128)(2,1)}, u32[]{:S(2)}) copy-start(bf16[512,512]{1,0:T(8,128)(2,1)} %value_ref.1) | copy-start | bytes 1572868
  23.4 1.0 %copy-start.2 = (bf16[512,512]{1,0:T(8,128)(2,1)S(1)}, bf16[512,512]{1,0:T(8,128)(2,1)}, u32[]{:S(2)}) copy-start(bf16[512,512]{1,0:T(8,128)(2,1)} %grad_ref.1) | copy-start | bytes 1572868
  24.4 0.9 copy-start.3
  25.4 0.9 copy-start.4
  26.3 0.7 copy-start.7
  45.7 21.0 %copy-start.8 = (bf16[64,16,128]{2,1,0:T(8,128)(2,1)S(1)}, bf16[64,16,128]{2,1,0:T(8,128)(2,1)}, u32[]{:S(2)}) copy-start(bf16[64,16,128]{2,1,0:T(8,128)(2,1)} %get-tuple-element.22) | copy-start | bytes 786436
  45.7 27.6 %collective-permute-start.1 = (bf16[64,16,128]{2,1,0:T(8,128)(2,1)}, bf16[64,16,128]{2,1,0:T(8,128)(2,1)}, u32[]{:S(2)}, u32[]{:S(2)}) collective-permute-start(bf16[64,16,128]{2,1,0:T(8,128)(2,1)} %get-tuple-element.22), channel_id=1, source_target_pairs={{0,4},{2,6},{4,0},{6,2},{1,5},{3,7},{5,1},{7,3},{8,12},{10,14},{12... | collective-permute-start | bytes 786440 | tf_op jit(solution)/shard_map/ppermute | solution.py:387
  50.8 18.4 %all-to-all-start.1 = ((bf16[64,8,128]{2,1,0:T(8,128)(2,1)}), bf16[64,8,128]{2,1,0:T(8,128)(2,1)S(1)}, u32[]{:S(2)}, u32[]{:S(2)}) async-start(bf16[64,8,128]{2,1,0:T(8,128)(2,1)} %bitcast.2), calls=%async_computation.1 | async-start | bytes 262144 | tf_op jit(solution)/shard_map/all_to_all | solution.py:377
  57.4 32.3 %collective-permute-start.2 = (bf16[64,16,128]{2,1,0:T(8,128)(2,1)}, bf16[64,16,128]{2,1,0:T(8,128)(2,1)}, u32[]{:S(2)}, u32[]{:S(2)}) collective-permute-start(bf16[64,16,128]{2,1,0:T(8,128)(2,1)} %get-tuple-element.22), channel_id=1, source_target_pairs={{0,2},{2,4},{4,6},{6,0},{1,3},{3,5},{5,7},{7,1},{8,10},{10,12},{12... | collective-permute-start | bytes 786440 | tf_op jit(solution)/shard_map/ppermute | solution.py:387
  59.9 30.8 %collective-permute-start.3 = (bf16[64,16,128]{2,1,0:T(8,128)(2,1)}, bf16[64,16,128]{2,1,0:T(8,128)(2,1)}, u32[]{:S(2)}, u32[]{:S(2)}) collective-permute-start(bf16[64,16,128]{2,1,0:T(8,128)(2,1)} %get-tuple-element.22), channel_id=1, source_target_pairs={{0,6},{2,0},{4,2},{6,4},{1,7},{3,1},{5,3},{7,5},{8,14},{10,8},{12,... | collective-permute-start | bytes 786440 | tf_op jit(solution)/shard_map/ppermute | solution.py:387
  64.5 37.6 %copy-start.5 = (f32[32,256]{1,0:T(8,128)S(1)}, f32[32,256]{1,0:T(8,128)}, u32[]{:S(2)}) copy-start(f32[32,256]{1,0:T(8,128)} %weight_ref.1) | copy-start | bytes 98308
  64.5 37.6 %copy-start.6 = (bf16[32,256]{1,0:T(8,128)(2,1)S(1)}, bf16[32,256]{1,0:T(8,128)(2,1)}, u32[]{:S(2)}) copy-start(bf16[32,256]{1,0:T(8,128)(2,1)} %get-tuple-element.23.own_ref) | copy-start | bytes 49156
  64.5 27.2 %collective-permute-start = (bf16[2048,128]{1,0:T(8,128)(2,1)S(1)}, bf16[2048,128]{1,0:T(8,128)(2,1)S(1)}, u32[]{:S(2)}, u32[]{:S(2)}) collective-permute-start(bf16[2048,128]{1,0:T(8,128)(2,1)S(1)} %bitcast.17), channel_id=1, source_target_pairs={{0,1},{1,0},{2,3},{3,2},{4,5},{5,4},{6,7},{7,6},{8,9},{9,8},{10,11... | collective-permute-start | bytes 1572872 | tf_op jit(solution)/shard_map/ppermute | solution.py:389
  69.9 8.7 %all-to-all-start.2 = ((f32[8,8,128]{2,1,0:T(8,128)}), f32[8,8,128]{2,1,0:T(8,128)S(1)}, u32[]{:S(2)}, u32[]{:S(2)}) async-start(f32[8,8,128]{2,1,0:T(8,128)} %summed.1), calls=%async_computation.2 | async-start | bytes 65536 | tf_op jit(solution)/shard_map/all_to_all | solution.py:378
  79.5 22.7 %all-to-all-start.3 = ((bf16[64,2,640]{2,1,0:T(2,128)(2,1)}), bf16[64,2,640]{2,1,0:T(2,128)(2,1)S(1)}, u32[]{:S(2)}, u32[]{:S(2)}) async-start(bf16[64,2,640]{2,1,0:T(2,128)(2,1)} %get-tuple-element.21), calls=%async_computation.3 | async-start | bytes 327680 | tf_op jit(solution)/shard_map/all_to_all | solution.py:382
